TPU v7x, 32 devices: a whole 2x2x4 slice. The times are simulated.
32 devices in a mesh: ep: 8 (over z, x), tp: 4 (over y, core).
Axes of the slice: x: 2, y: 2, z: 4, core: 2. Of those that a mesh axis runs over, the one named last changes fastest.
Arguments:
- mixer_input: bfloat16 [5120, 2048], P('ep'), may hold values from -6 to 6
- mixer_gain: float32 [2048], replicated, may hold values from 0.1 to 1.9
- value_weight: bfloat16 [2048, 1024], P(None, 'tp'), may hold values from -0.125 to 0.125
- inner_gate: bfloat16 [2048, 1024], P(None, 'tp'), may hold values from -0.125 to 0.125
- outer_gate: bfloat16 [2048, 1024], P(None, 'tp'), may hold values from -0.125 to 0.125
- kernel_taps: float32 [3, 1024], P(None, 'tp'), may hold values from -3 to 3
- mixer_proj: bfloat16 [1024, 2048], P('tp'), may hold values from -0.1875 to 0.1875
- expert_input: bfloat16 [5120, 2048], P(('ep', 'tp')), may hold values from -6 to 6
- expert_gain: float32 [2048], replicated, may hold values from 0.1 to 1.9
- routes: int32 [5120, 2], P(('ep', 'tp')), may hold values from 0 to 7, as said below
- group_logits: float32 [5120, 1], P(('ep', 'tp')), may hold values from -6 to 6
- pair_logits: float32 [5120, 2], P(('ep', 'tp')), may hold values from -6 to 6
- gate_weight: bfloat16 [8, 2048, 1024], P('ep', None, 'tp'), may hold values from -0.125 to 0.125
- up_weight: bfloat16 [8, 2048, 1024], P('ep', None, 'tp'), may hold values from -0.125 to 0.125
- down_weight: bfloat16 [8, 1024, 2048], P('ep', 'tp'), may hold values from -0.75 to 0.75
Outputs:
- mixer_output: bfloat16 [5120, 2048], P(('ep', 'tp'))
- expert_output: bfloat16 [5120, 2048], P(('ep', 'tp'))
Inputs may be any that keep to these rules, and one draw needn't show every extreme that they name: `routes`: both entries of a row are different experts of one group (equal after integer division by 8). In the rows of one device every group is chosen by the same number of rows, no expert is named more than 80 times, and in every draw one expert is named exactly 80 times in the rows of every device.
All inputs are finite; a program needn't handle non-finite values.
Results may differ from a plain program's by a relative error of at most 0.01.
Values may be sent and summed in bfloat16 or wider, within the bound.
No kernel may reach another device: no remote copies, remote signals or barrier semaphores. Data moves between devices by JAX's collectives and lax.ppermute only.
A program may use at most 128 MiB of HBM per device.

v0:
```python
import jax
import jax.numpy as jnp
from jax import lax
from jax.experimental import pallas as pl
from jax.experimental.pallas import tpu as pltpu
from jax.sharding import PartitionSpec as P


EPG = 8
EPSILON = 1e-06


def swapped(value, axis, bit):
    count = lax.axis_size(axis)
    return lax.ppermute(value, axis, [(i, i ^ bit) for i in range(count)])


def call(body, outs, *operands, scratch=(), smem=0, aliases=None):
    vmem = pl.BlockSpec(memory_space=pltpu.VMEM)
    scalar = pl.BlockSpec(memory_space=pltpu.SMEM)
    single = not isinstance(outs, (list, tuple))
    return pl.pallas_call(
        body,
        out_shape=outs if single else list(outs),
        in_specs=[scalar] * smem + [vmem] * (len(operands) - smem),
        out_specs=vmem if single else [vmem] * len(outs),
        scratch_shapes=list(scratch),
        input_output_aliases=aliases or {},
    )(*operands)


def slots_of(experts, capacity, me, routes_ref):
    first, second = routes_ref[0:1, :], routes_ref[1:2, :]
    local = first.shape[1]
    expert = lax.broadcasted_iota(jnp.int32, (experts, local), 0)
    hit_first = jnp.where(expert == first, 1.0, 0.0)
    hit_second = jnp.where(expert == second, 1.0, 0.0)
    row = lax.broadcasted_iota(jnp.int32, (local, local), 0)
    column = lax.broadcasted_iota(jnp.int32, (local, local), 1)
    earlier = jnp.where(row < column, 1.0, 0.0).astype(jnp.bfloat16)
    before_first = jnp.dot(hit_first.astype(jnp.bfloat16), earlier, preferred_element_type=jnp.float32)
    before_second = jnp.dot(hit_second.astype(jnp.bfloat16), earlier, preferred_element_type=jnp.float32)
    before_second = before_second + jnp.sum(hit_first, axis=1, keepdims=True)
    rank_first = jnp.sum(hit_first * before_first, axis=0, keepdims=True).astype(jnp.int32)
    rank_second = jnp.sum(hit_second * before_second, axis=0, keepdims=True).astype(jnp.int32)
    slot = lax.broadcasted_iota(jnp.int32, (experts * capacity, local), 0)
    is_first = slot == (first ^ me) * capacity + rank_first
    is_second = slot == (second ^ me) * capacity + rank_second
    return is_first, is_second


def dispatch_kernel(experts, capacity, me_ref, rows_ref, gain_ref, routes_ref, *blocks):
    is_first, is_second = slots_of(experts, capacity, me_ref[0], routes_ref)
    place = jnp.where(is_first | is_second, 1.0, 0.0).astype(jnp.bfloat16)
    wide = rows_ref[...].astype(jnp.float32)
    scale = lax.rsqrt(jnp.mean(wide * wide, axis=-1, keepdims=True) + EPSILON)
    norm = (wide * scale * gain_ref[...]).astype(jnp.bfloat16)
    placed = jnp.dot(place, norm, preferred_element_type=jnp.float32).astype(jnp.bfloat16)
    height = placed.shape[0] // len(blocks)
    for i, block in enumerate(blocks):
        block[...] = placed[i * height : (i + 1) * height]


def share_kernel(experts, capacity, heights, me_ref, routes_ref, group_ref, pair_ref, *outs):
    is_first, is_second = slots_of(experts, capacity, me_ref[0], routes_ref)
    logits = group_ref[...]
    first = routes_ref[0:1, :]
    group = lax.broadcasted_iota(jnp.int32, logits.shape, 0)
    chosen = (group * EPG <= first) & (first < group * EPG + EPG)
    picked = jnp.sum(jnp.where(chosen, logits, 0.0), axis=0, keepdims=True)
    group_weight = 1.0 / jnp.sum(jnp.exp(logits - picked), axis=0, keepdims=True)
    apart = pair_ref[0:1, :] - pair_ref[1:2, :]
    weight_first = group_weight / (1.0 + jnp.exp(-apart))
    weight_second = group_weight / (1.0 + jnp.exp(apart))
    weights = jnp.where(is_first, weight_first, 0.0) + jnp.where(is_second, weight_second, 0.0)
    start = 0
    for i, height in enumerate(heights):
        share = weights[start : start + height].T
        high = share.astype(jnp.bfloat16)
        outs[2 * i][...] = high
        outs[2 * i + 1][...] = (share - high.astype(jnp.float32)).astype(jnp.bfloat16)
        start += height


def hidden_kernel(blocks, split, *refs):
    out_ref = refs[-1]
    rows = jnp.concatenate([r[...] for r in refs[:blocks]], axis=0)
    gates = refs[blocks : blocks + split]
    uppers = refs[blocks + split : blocks + 2 * split]
    width = gates[0].shape[1]
    for k in range(split):
        first = jnp.dot(rows, gates[k][...], preferred_element_type=jnp.float32)
        second = jnp.dot(rows, uppers[k][...], preferred_element_type=jnp.float32)
        value = first / (1.0 + jnp.exp(-first)) * second
        out_ref[:, k * width : (k + 1) * width] = value.astype(jnp.bfloat16)


def down_kernel(split, *refs):
    hidden_ref = refs[0]
    downs = refs[1 : 1 + split]
    outs = refs[1 + split :]
    width = downs[0].shape[0]
    total = None
    for k in range(split):
        part = jnp.dot(
            hidden_ref[:, k * width : (k + 1) * width], downs[k][...], preferred_element_type=jnp.float32
        )
        total = part if total is None else total + part
    answer = total.astype(jnp.bfloat16)
    height = answer.shape[0] // len(outs)
    for i, out in enumerate(outs):
        out[...] = answer[i * height : (i + 1) * height]


def combine_kernel(blocks, high_ref, low_ref, *refs):
    out_ref = refs[-1]
    rows = jnp.concatenate([r[...] for r in refs[:blocks]], axis=0)
    total = jnp.dot(high_ref[...], rows, preferred_element_type=jnp.float32)
    total = total + jnp.dot(low_ref[...], rows, preferred_element_type=jnp.float32)
    if len(refs) > blocks + 1:
        total = total + refs[blocks][...]
    out_ref[...] = total.astype(out_ref.dtype)


def mixer_a_kernel(rows_ref, gain_ref, value_ref, inner_ref, outer_ref, mixed_ref, gate_ref, top_ref, bottom_ref):
    wide = rows_ref[...].astype(jnp.float32)
    scale = lax.rsqrt(jnp.mean(wide * wide, axis=-1, keepdims=True) + EPSILON)
    norm = (wide * scale * gain_ref[...]).astype(jnp.bfloat16)
    value = jnp.dot(norm, value_ref[...], preferred_element_type=jnp.float32)
    inner = jnp.dot(norm, inner_ref[...], preferred_element_type=jnp.float32)
    gate_ref[...] = jnp.dot(norm, outer_ref[...], preferred_element_type=jnp.float32)
    mixed = inner * value
    mixed_ref[...] = mixed.astype(jnp.bfloat16)
    count = mixed.shape[0]

    @pl.when(pl.program_id(0) == 0)
    def _():
        top_ref[...] = mixed[:1].astype(jnp.bfloat16)

    @pl.when(pl.program_id(0) == pl.num_programs(0) - 1)
    def _():
        bottom_ref[...] = mixed[count - 1 :].astype(jnp.bfloat16)


def mixer_a(rows, gain, value_weight, inner_gate, outer_gate, steps):
    total, width = rows.shape
    channels = value_weight.shape[1]
    height = total // steps
    whole = pl.BlockSpec((width, channels), lambda i: (0, 0))
    edge = pl.BlockSpec((1, channels), lambda i: (0, 0))
    piece = pl.BlockSpec((height, channels), lambda i: (i, 0))
    return pl.pallas_call(
        mixer_a_kernel,
        grid=(steps,),
        out_shape=[
            jax.ShapeDtypeStruct((total, channels), jnp.bfloat16),
            jax.ShapeDtypeStruct((total, channels), jnp.float32),
            jax.ShapeDtypeStruct((1, channels), jnp.bfloat16),
            jax.ShapeDtypeStruct((1, channels), jnp.bfloat16),
        ],
        in_specs=[
            pl.BlockSpec((height, width), lambda i: (i, 0)),
            pl.BlockSpec((1, width), lambda i: (0, 0)),
            whole,
            whole,
            whole,
        ],
        out_specs=[piece, piece, edge, edge],
        name="mixer_a",
    )(rows, gain.reshape(1, width), value_weight, inner_gate, outer_gate)


def mixer_b_kernel(split, me_ref, mixed_ref, gate_ref, above_ref, below_ref, taps_ref, proj_ref, *refs):
    rows_ref = refs[-1]
    outs = refs[:-1]
    mixed = mixed_ref[...].astype(jnp.float32)
    count = mixed.shape[0]
    place = lax.broadcasted_iota(jnp.int32, mixed.shape, 0)
    before = jnp.where(place == 0, above_ref[...].astype(jnp.float32), pltpu.roll(mixed, 1, 0))
    after = jnp.where(place == count - 1, below_ref[...].astype(jnp.float32), pltpu.roll(mixed, count - 1, 0))
    summed = taps_ref[0:1, :] * before + taps_ref[1:2, :] * mixed + taps_ref[2:3, :] * after
    rows_ref[...] = (gate_ref[...] * summed).astype(jnp.bfloat16)
    owned = count // split
    for k, out in enumerate(outs):
        start = pl.multiple_of((me_ref[0] ^ k) * owned, owned)
        part = jnp.dot(rows_ref[pl.ds(start, owned), :], proj_ref[...], preferred_element_type=jnp.float32)
        out[...] = part.astype(out.dtype)


def add_kernel(*refs):
    total = refs[0][...].astype(jnp.float32)
    for ref in refs[1:-1]:
        total = total + ref[...].astype(jnp.float32)
    refs[-1][...] = total.astype(refs[-1].dtype)


def gathered_blocks(piece, axis):
    count = lax.axis_size(axis)
    blocks = [piece]
    for k in range(1, count):
        low = k & -k
        blocks.append(swapped(blocks[k ^ low], axis, low))
    return blocks


def on_device(
    mixer_input,
    mixer_gain,
    value_weight,
    inner_gate,
    outer_gate,
    kernel_taps,
    mixer_proj,
    expert_input,
    expert_gain,
    routes,
    group_logits,
    pair_logits,
    gate_weight,
    up_weight,
    down_weight,
):
    experts = lax.axis_size("ep")
    split = lax.axis_size("tp")
    local, width = expert_input.shape
    capacity = 4 * local // experts
    slots = experts * capacity
    direct = experts == 8
    height = capacity if direct else slots
    count = slots // height
    bf16, f32 = jnp.bfloat16, jnp.float32
    shaped = jax.ShapeDtypeStruct
    me_tp = lax.axis_index("tp").astype(jnp.int32).reshape(1)
    me_ep = lax.axis_index("ep").astype(jnp.int32)
    me_ep = (me_ep if direct else jnp.zeros((), jnp.int32)).reshape(1)

    gates = gathered_blocks(gate_weight[0], "tp")
    uppers = gathered_blocks(up_weight[0], "tp")
    downs = gathered_blocks(down_weight[0], "tp")

    outgoing = call(
        lambda *refs: dispatch_kernel(experts, capacity, *refs),
        [shaped((height, width), bf16)] * count,
        me_ep,
        expert_input,
        expert_gain.reshape(1, width),
        routes.T,
        smem=1,
    )

    def exchanged(value):
        rows = value.reshape(experts, capacity, width)
        return lax.all_to_all(rows, "ep", split_axis=0, concat_axis=0, tiled=True).reshape(slots, width)

    if direct:
        arrived = [outgoing[0]] + [swapped(outgoing[d], "ep", d) for d in range(1, count)]
        groups = (("near", range(0, 4)), ("far_b", range(6, 8)), ("far_a", range(4, 6)))
    else:
        arrived = [exchanged(outgoing[0])]
        groups = (("near", range(1)),)

    mixed, gate, top, bottom = mixer_a(mixer_input, mixer_gain, value_weight, inner_gate, outer_gate, split)
    last = experts - 1
    above = lax.ppermute(bottom, "ep", [(i, i + 1) for i in range(last)])
    below = lax.ppermute(top, "ep", [(i + 1, i) for i in range(last)])

    ordered = sorted(groups, key=lambda g: g[1][0])
    heights = [len(members) * height for _, members in ordered]
    shares = call(
        lambda *refs: share_kernel(experts, capacity, heights, *refs),
        [shaped((local, h), bf16) for h in heights for _ in range(2)],
        me_ep,
        routes.T,
        group_logits.T,
        pair_logits.T,
        smem=1,
    )
    shares = {name: shares[2 * i : 2 * i + 2] for i, (name, _) in enumerate(ordered)}

    back = {}
    units = split * gate_weight.shape[2]
    for name, members in groups:
        n = len(members)
        hidden = call(
            lambda *refs, n=n: hidden_kernel(n, split, *refs),
            shaped((n * height, units), bf16),
            *[arrived[d] for d in members],
            *gates,
            *uppers,
        )
        answers = call(lambda *refs: down_kernel(split, *refs), [shaped((height, width), bf16)] * n, hidden, *downs)
        for d, answer in zip(members, answers):
            if not direct:
                back[d] = exchanged(answer)
            else:
                back[d] = swapped(answer, "ep", d) if d else answer

    owned = mixed.shape[0] // split
    parts = call(
        lambda *refs: mixer_b_kernel(split, *refs),
        [shaped((owned, width), bf16 if k % 2 else f32) for k in range(split)],
        me_tp,
        mixed,
        gate,
        above,
        below,
        kernel_taps,
        mixer_proj,
        scratch=[pltpu.VMEM(mixed.shape, bf16)],
        smem=1,
    )
    addends = [[part] for part in parts]
    bit = 1
    while bit < split:
        for k in reversed(range(bit, split, 2 * bit)):
            value = addends[k][0]
            if bit > 1:
                value = call(add_kernel, shaped((owned, width), bf16), *addends[k])
            addends[k - bit].append(swapped(value, "tp", bit))
        bit *= 2
    mixer_output = call(add_kernel, shaped((owned, width), bf16), *addends[0])

    total = []
    for i, (name, members) in enumerate(groups):
        kind = bf16 if i == len(groups) - 1 else f32
        blocks = [back[d] for d in members]
        total = [
            call(
                lambda *refs, n=len(blocks): combine_kernel(n, *refs),
                shaped((local, width), kind),
                *shares[name],
                *blocks,
                *total,
            )
        ]
    return (mixer_output, total[0])


def solution(mesh):
    in_specs = (
        P("ep", None),
        P(),
        P(None, "tp"),
        P(None, "tp"),
        P(None, "tp"),
        P(None, "tp"),
        P("tp", None),
        P(("ep", "tp"), None),
        P(),
        P(("ep", "tp"), None),
        P(("ep", "tp"), None),
        P(("ep", "tp"), None),
        P("ep", None, "tp"),
        P("ep", None, "tp"),
        P("ep", "tp", None),
    )
    out_specs = (P(("ep", "tp"), None), P(("ep", "tp"), None))

    return jax.shard_map(on_device, mesh=mesh, in_specs=in_specs, out_specs=out_specs, check_vma=False)
```

profile of v0, /device:TPU:0, one launch (start us, length us, event | category | flops | bytes accessed | tf_op | source)
XLA Modules:
  0.0 222.2 jit_solution(1563942009448933500)
XLA Ops:
  0.6 3.5 %shard_map.162 = (bf16[80,2048]{1,0:T(8,128)(2,1)}, bf16[80,2048]{1,0:T(8,128)(2,1)}, bf16[80,2048]{1,0:T(8,128)(2,1)}, bf16[80,2048]{1,0:T(8,128)(2,1)}, bf16[8...) custom-call(s32[1]{0:T(128)} %bitcast.2.refs_0_, ...), custom_call_target="tpu_custom_call" | custom-call | tf_op jit(solution)/shard_map/pallas_call | solution.py:22
  4.1 4.1 %collective-permute-start.5 = (bf16[80,2048]{1,0:T(8,128)(2,1)}, bf16[80,2048]{1,0:T(8,128)(2,1)S(1)}, u32[]{:S(2)}, u32[]{:S(2)}) collective-permute-start(bf16[80,2048]{1,0:T(8,128)(2,1)} %get-tuple-element.42), channel_id=1, source_target_pairs={{0,16},{4,20},{8,24},{12,28},{16,0},{20,4},{24,8},{28,12},{1,17},{... | collective-permute-start | bytes 983048 | tf_op jit(solution)/shard_map/ppermute | solution.py:15
  9.7 6.7 %mixer_a.1 = (bf16[640,256]{1,0:T(8,128)(2,1)}, f32[640,256]{1,0:T(8,128)}, bf16[1,256]{1,0:T(2,128)(2,1)}, bf16[1,256]{1,0:T(2,128)(2,1)}) custom-call(bf16[640,2048]{1,0:T(8,128)(2,1)} %rows_ref.1, f32[1,2048]{1,0:T(1,128)} %bitcast.26, bf16[2048,256]{1,0:T(8,128)(2,1)} %value_ref.1, bf16[2048,256]{1,0:T(8,128)(2,1)} %inner_ref.1, bf16[2048,256]{1,0:T(8,128)(2,1)} %outer_ref.1), custom_call_target="tpu_custom_call" | custom-call | tf_op jit(solution)/shard_map/mixer_a/pallas_call | solution.py:152
  16.4 2.4 %collective-permute-start = (bf16[1,256]{1,0:T(2,128)(2,1)}, bf16[1,256]{1,0:T(2,128)(2,1)S(1)}, u32[]{:S(2)}, u32[]{:S(2)}) collective-permute-start(bf16[1,256]{1,0:T(2,128)(2,1)} %get-tuple-element.34), channel_id=1, source_target_pairs={{0,4},{4,8},{8,12},{12,16},{16,20},{20,24},{24,28},{1,5},{5,9},{9,... | collective-permute-start | bytes 1544 | tf_op jit(solution)/shard_map/ppermute | solution.py:264
  20.2 4.7 %collective-permute-start.23 = (bf16[80,2048]{1,0:T(8,128)(2,1)}, bf16[80,2048]{1,0:T(8,128)(2,1)S(1)}, u32[]{:S(2)}, u32[]{:S(2)}) collective-permute-start(bf16[80,2048]{1,0:T(8,128)(2,1)} %get-tuple-element.56), channel_id=1, source_target_pairs={{0,8},{4,12},{8,0},{12,4},{16,24},{20,28},{24,16},{28,20},{1,9},{5... | collective-permute-start | bytes 983048 | tf_op jit(solution)/shard_map/ppermute | solution.py:15
  28.8 4.8 %collective-permute-done.23.refs_2_ = bf16[80,2048]{1,0:T(8,128)(2,1)S(1)} collective-permute-done((bf16[80,2048]{1,0:T(8,128)(2,1)}, bf16[80,2048]{1,0:T(8,128)(2,1)S(1)}, u32[]{:S(2)}, u32[]{:S(2)}) %collective-permute-start.23) | collective-permute-done | bytes 327712 | tf_op jit(solution)/shard_map/ppermute | solution.py:15
  35.9 4.3 %shard_map.158 = (f32[160,2048]{1,0:T(8,128)}, bf16[160,2048]{1,0:T(8,128)(2,1)}, f32[160,2048]{1,0:T(8,128)}, bf16[160,2048]{1,0:T(8,128)(2,1)}) custom-call(s32[1]{0:T(128)} %bitcast.refs_0_, bf16[640,256]{1,0:T(8,128)(2,1)} %get-tuple-element.32.refs_1_, f32[640,256]{1,0:T(8,128)} %get-tuple-element.33.refs_2_, bf16[1,256]{1,0:T(2,128)(2,1)} %copy-done.18, ...), custom_call_target="tpu_custom_call" | custom-call | tf_op jit(solution)/shard_map/pallas_call | solution.py:22
  40.2 2.3 %collective-permute-done.3.refs_1_ = bf16[160,2048]{1,0:T(8,128)(2,1)S(1)} collective-permute-done((bf16[160,2048]{1,0:T(8,128)(2,1)}, bf16[160,2048]{1,0:T(8,128)(2,1)S(1)}, u32[]{:S(2)}, u32[]{:S(2)}) %collective-permute-start.3) | collective-permute-done | bytes 655392 | tf_op jit(solution)/shard_map/ppermute | solution.py:15
  43.0 8.2 %collective-permute-done.8.refs_4_.refs_6_ = bf16[2048,256]{1,0:T(8,128)(2,1)} collective-permute-done((bf16[2048,256]{1,0:T(8,128)(2,1)S(1)}, bf16[2048,256]{1,0:T(8,128)(2,1)}, u32[]{:S(2)}, u32[]{:S(2)}) %collective-permute-start.8) | collective-permute-done | bytes 1048608 | tf_op jit(solution)/shard_map/ppermute | solution.py:15
  51.2 22.5 %collective-permute-done.11.refs_8_.refs_10_ = bf16[2048,256]{1,0:T(8,128)(2,1)} collective-permute-done((bf16[2048,256]{1,0:T(8,128)(2,1)S(1)}, bf16[2048,256]{1,0:T(8,128)(2,1)}, u32[]{:S(2)}, u32[]{:S(2)}) %collective-permute-start.11) | collective-permute-done | bytes 1048608 | tf_op jit(solution)/shard_map/ppermute | solution.py:15
  73.7 21.9 %collective-permute-done.14.refs_3_ = bf16[256,2048]{1,0:T(8,128)(2,1)} collective-permute-done((bf16[256,2048]{1,0:T(8,128)(2,1)S(1)}, bf16[256,2048]{1,0:T(8,128)(2,1)}, u32[]{:S(2)}, u32[]{:S(2)}) %collective-permute-start.14) | collective-permute-done | bytes 1048608 | tf_op jit(solution)/shard_map/ppermute | solution.py:15
  95.5 2.4 %shard_map.159 = bf16[160,2048]{1,0:T(8,128)(2,1)} custom-call(f32[160,2048]{1,0:T(8,128)} %get-tuple-element.38.refs_0_, bf16[160,2048]{1,0:T(8,128)(2,1)} %copy-done.4), custom_call_target="tpu_custom_call" | custom-call | tf_op jit(solution)/shard_map/pallas_call | solution.py:22
  100.2 2.2 %collective-permute-start.18 = (bf16[80,2048]{1,0:T(8,128)(2,1)}, bf16[80,2048]{1,0:T(8,128)(2,1)S(1)}, u32[]{:S(2)}, u32[]{:S(2)}) collective-permute-start(bf16[80,2048]{1,0:T(8,128)(2,1)} %get-tuple-element.48), channel_id=1, source_target_pairs={{0,24},{4,28},{8,16},{12,20},{16,8},{20,12},{24,0},{28,4},{1,25},{... | collective-permute-start | bytes 983048 | tf_op jit(solution)/shard_map/ppermute | solution.py:15
  102.4 4.2 %collective-permute-start.19 = (bf16[80,2048]{1,0:T(8,128)(2,1)}, bf16[80,2048]{1,0:T(8,128)(2,1)S(1)}, u32[]{:S(2)}, u32[]{:S(2)}) collective-permute-start(bf16[80,2048]{1,0:T(8,128)(2,1)} %get-tuple-element.49), channel_id=1, source_target_pairs={{0,28},{4,24},{8,20},{12,16},{16,12},{20,8},{24,4},{28,0},{1,29},{... | collective-permute-start | bytes 983048 | tf_op jit(solution)/shard_map/ppermute | solution.py:15
  106.6 7.5 %shard_map.167.refs_0_ = bf16[320,1024]{1,0:T(8,128)(2,1)} custom-call(bf16[80,2048]{1,0:T(8,128)(2,1)} %get-tuple-element.54.refs_0_, bf16[80,2048]{1,0:T(8,128)(2,1)} %collective-permute-done.22.refs_1_, bf16[80,2048]{1,0:T(8,128)(2,1)} %copy-done.8, bf16[80,2048]{1,0:T(8,128)(2,1)} %collective-permute-done.24.refs_3_, bf16[2048,256]{1,0:T(8,128)(2,1)} %bitcast.10, ...), custom_call_target="tpu_custom_call" | custom-call | tf_op jit(solution)/shard_map/pallas_call | solution.py:22
  114.1 4.9 %shard_map.168 = (bf16[80,2048]{1,0:T(8,128)(2,1)}, bf16[80,2048]{1,0:T(8,128)(2,1)}, bf16[80,2048]{1,0:T(8,128)(2,1)}, bf16[80,2048]{1,0:T(8,128)(2,1)}) custom-call(bf16[320,1024]{1,0:T(8,128)(2,1)} %shard_map.167.refs_0_, bf16[256,2048]{1,0:T(8,128)(2,1)} %bitcast.20, bf16[256,2048]{1,0:T(8,128)(2,1)} %collective-permute-done.13.refs_2_, ...), custom_call_target="tpu_custom_call" | custom-call | tf_op jit(solution)/shard_map/pallas_call | solution.py:22
  119.0 13.0 %collective-permute-done.6.refs_1_ = bf16[80,2048]{1,0:T(8,128)(2,1)S(1)} collective-permute-done((bf16[80,2048]{1,0:T(8,128)(2,1)}, bf16[80,2048]{1,0:T(8,128)(2,1)S(1)}, u32[]{:S(2)}, u32[]{:S(2)}) %collective-permute-start.6) | collective-permute-done | bytes 327712 | tf_op jit(solution)/shard_map/ppermute | solution.py:15
  132.6 6.1 %collective-permute-start.26 = (bf16[80,2048]{1,0:T(8,128)(2,1)}, bf16[80,2048]{1,0:T(8,128)(2,1)S(1)}, u32[]{:S(2)}, u32[]{:S(2)}) collective-permute-start(bf16[80,2048]{1,0:T(8,128)(2,1)} %get-tuple-element.60), channel_id=1, source_target_pairs={{0,8},{4,12},{8,0},{12,4},{16,24},{20,28},{24,16},{28,20},{1,9},{5... | collective-permute-start | bytes 983048 | tf_op jit(solution)/shard_map/ppermute | solution.py:15
  138.8 5.9 %shard_map.163.refs_0_ = bf16[160,1024]{1,0:T(8,128)(2,1)} custom-call(bf16[80,2048]{1,0:T(8,128)(2,1)} %copy-done.7, bf16[80,2048]{1,0:T(8,128)(2,1)} %copy-done.11, bf16[2048,256]{1,0:T(8,128)(2,1)} %bitcast.11, bf16[2048,256]{1,0:T(8,128)(2,1)} %collective-permute-done.7.refs_3_.refs_5_, bf16[2048,256]{1,0:T(8,128)(2,1)} %collective-permute-done.8.refs_4_.refs_6_, ...), custom_call_target="tpu_custom_call" | custom-call | tf_op jit(solution)/shard_map/pallas_call | solution.py:22
  144.6 3.9 %shard_map.164 = (bf16[80,2048]{1,0:T(8,128)(2,1)}, bf16[80,2048]{1,0:T(8,128)(2,1)}) custom-call(bf16[160,1024]{1,0:T(8,128)(2,1)} %shard_map.163.refs_0_, bf16[256,2048]{1,0:T(8,128)(2,1)} %bitcast.21, bf16[256,2048]{1,0:T(8,128)(2,1)} %collective-permute-done.13.refs_2_, bf16[256,2048]{1,0:T(8,128)(2,1)} %collective-permute-done.14.refs_3_, ...), custom_call_target="tpu_custom_call" | custom-call | tf_op jit(solution)/shard_map/pallas_call | solution.py:22
  149.6 5.9 %shard_map.165.refs_0_ = bf16[160,1024]{1,0:T(8,128)(2,1)} custom-call(bf16[80,2048]{1,0:T(8,128)(2,1)} %copy-done.9, bf16[80,2048]{1,0:T(8,128)(2,1)} %copy-done.10, bf16[2048,256]{1,0:T(8,128)(2,1)} %bitcast.12, bf16[2048,256]{1,0:T(8,128)(2,1)} %collective-permute-done.7.refs_3_.refs_5_, bf16[2048,256]{1,0:T(8,128)(2,1)} %collective-permute-done.8.refs_4_.refs_6_, ...), custom_call_target="tpu_custom_call" | custom-call | tf_op jit(solution)/shard_map/pallas_call | solution.py:22
  155.5 4.0 %shard_map.166 = (bf16[80,2048]{1,0:T(8,128)(2,1)}, bf16[80,2048]{1,0:T(8,128)(2,1)}) custom-call(bf16[160,1024]{1,0:T(8,128)(2,1)} %shard_map.165.refs_0_, bf16[256,2048]{1,0:T(8,128)(2,1)} %bitcast.22, bf16[256,2048]{1,0:T(8,128)(2,1)} %collective-permute-done.13.refs_2_, bf16[256,2048]{1,0:T(8,128)(2,1)} %collective-permute-done.14.refs_3_, ...), custom_call_target="tpu_custom_call" | custom-call | tf_op jit(solution)/shard_map/pallas_call | solution.py:22
  161.3 2.6 %collective-permute-start.21 = (bf16[80,2048]{1,0:T(8,128)(2,1)}, bf16[80,2048]{1,0:T(8,128)(2,1)S(1)}, u32[]{:S(2)}, u32[]{:S(2)}) collective-permute-start(bf16[80,2048]{1,0:T(8,128)(2,1)} %get-tuple-element.51), channel_id=1, source_target_pairs={{0,28},{4,24},{8,20},{12,16},{16,12},{20,8},{24,4},{28,0},{1,29},{... | collective-permute-start | bytes 983048 | tf_op jit(solution)/shard_map/ppermute | solution.py:15
  163.9 3.2 %collective-permute-start.17 = (bf16[80,2048]{1,0:T(8,128)(2,1)}, bf16[80,2048]{1,0:T(8,128)(2,1)}, u32[]{:S(2)}, u32[]{:S(2)}) collective-permute-start(bf16[80,2048]{1,0:T(8,128)(2,1)} %get-tuple-element.45), channel_id=1, source_target_pairs={{0,20},{4,16},{8,28},{12,24},{16,4},{20,0},{24,12},{28,8},{1,21},{... | collective-permute-start | bytes 983048 | tf_op jit(solution)/shard_map/ppermute | solution.py:15
  167.2 1.9 shard_map.161
  169.1 2.7 %shard_map.160 = bf16[160,2048]{1,0:T(8,128)(2,1)} custom-call(f32[160,2048]{1,0:T(8,128)} %get-tuple-element.36.refs_0_, bf16[160,2048]{1,0:T(8,128)(2,1)} %copy-done.5, bf16[160,2048]{1,0:T(8,128)(2,1)} %copy-done.6), custom_call_target="tpu_custom_call" | custom-call | tf_op jit(solution)/shard_map/pallas_call | solution.py:22
  172.5 3.4 %shard_map.169.refs_4_ = f32[160,2048]{1,0:T(8,128)} custom-call(bf16[160,320]{1,0:T(8,128)(2,1)} %get-tuple-element.52.refs_0_, bf16[160,320]{1,0:T(8,128)(2,1)} %get-tuple-element.53.refs_1_, bf16[80,2048]{1,0:T(8,128)(2,1)} %get-tuple-element.58.refs_2_, bf16[80,2048]{1,0:T(8,128)(2,1)} %copy-done.12, bf16[80,2048]{1,0:T(8,128)(2,1)} %copy-done.13, ...), custom_call_target="tpu_custom_call" | custom-call | tf_op jit(solution)/shard_map/pallas_call | solution.py:22
  175.9 3.8 %collective-permute-done.21.refs_3_ = bf16[80,2048]{1,0:T(8,128)(2,1)S(1)} collective-permute-done((bf16[80,2048]{1,0:T(8,128)(2,1)}, bf16[80,2048]{1,0:T(8,128)(2,1)S(1)}, u32[]{:S(2)}, u32[]{:S(2)}) %collective-permute-start.21) | collective-permute-done | bytes 327712 | tf_op jit(solution)/shard_map/ppermute | solution.py:15
  180.5 3.2 %shard_map.170.refs_4_ = f32[160,2048]{1,0:T(8,128)} custom-call(bf16[160,160]{1,0:T(8,128)(2,1)} %get-tuple-element.46.refs_0_, bf16[160,160]{1,0:T(8,128)(2,1)} %get-tuple-element.47.refs_1_, bf16[80,2048]{1,0:T(8,128)(2,1)} %copy-done.15, bf16[80,2048]{1,0:T(8,128)(2,1)} %copy-done.17, f32[160,2048]{1,0:T(8,128)} %shard_map.169.refs_4_), custom_call_target="tpu_custom_call" | custom-call | tf_op jit(solution)/shard_map/pallas_call | solution.py:22
  183.6 29.4 %collective-permute-done.16.refs_2_ = bf16[80,2048]{1,0:T(8,128)(2,1)S(1)} collective-permute-done((bf16[80,2048]{1,0:T(8,128)(2,1)}, bf16[80,2048]{1,0:T(8,128)(2,1)S(1)}, u32[]{:S(2)}, u32[]{:S(2)}) %collective-permute-start.16) | collective-permute-done | bytes 327712 | tf_op jit(solution)/shard_map/ppermute | solution.py:15
  213.0 6.3 %collective-permute-done.17.refs_3_ = bf16[80,2048]{1,0:T(8,128)(2,1)} collective-permute-done((bf16[80,2048]{1,0:T(8,128)(2,1)}, bf16[80,2048]{1,0:T(8,128)(2,1)}, u32[]{:S(2)}, u32[]{:S(2)}) %collective-permute-start.17) | collective-permute-done | bytes 327712 | tf_op jit(solution)/shard_map/ppermute | solution.py:15
  219.3 2.9 %shard_map.171 = bf16[160,2048]{1,0:T(8,128)(2,1)} custom-call(bf16[160,160]{1,0:T(8,128)(2,1)} %get-tuple-element.40.refs_0_, bf16[160,160]{1,0:T(8,128)(2,1)} %get-tuple-element.41.refs_1_, bf16[80,2048]{1,0:T(8,128)(2,1)} %copy-done.16, bf16[80,2048]{1,0:T(8,128)(2,1)} %collective-permute-done.17.refs_3_, f32[160,2048]{1,0:T(8,128)} %shard_map.170.refs_4_), custom_call_target="tpu_custom_call" | custom-call | tf_op jit(solution)/shard_map/pallas_call | solution.py:22
  (79 shorter events, 16.7 us)
Async XLA Ops:
  4.1 22.5 %collective-permute-start.5 = (bf16[80,2048]{1,0:T(8,128)(2,1)}, bf16[80,2048]{1,0:T(8,128)(2,1)S(1)}, u32[]{:S(2)}, u32[]{:S(2)}) collective-permute-start(bf16[80,2048]{1,0:T(8,128)(2,1)} %get-tuple-element.42), channel_id=1, source_target_pairs={{0,16},{4,20},{8,24},{12,28},{16,0},{20,4},{24,8},{28,12},{1,17},{... | collective-permute-start | bytes 983048 | tf_op jit(solution)/shard_map/ppermute | solution.py:15
  8.2 19.0 %collective-permute-start.22 = (bf16[80,2048]{1,0:T(8,128)(2,1)}, bf16[80,2048]{1,0:T(8,128)(2,1)}, u32[]{:S(2)}, u32[]{:S(2)}) collective-permute-start(bf16[80,2048]{1,0:T(8,128)(2,1)} %get-tuple-element.55), channel_id=1, source_target_pairs={{0,4},{4,0},{8,12},{12,8},{16,20},{20,16},{24,28},{28,24},{1,5},{5... | collective-permute-start | bytes 983048 | tf_op jit(solution)/shard_map/ppermute | solution.py:15
  9.7 16.9 %copy-start.1 = (bf16[1,2048,256]{2,1,0:T(8,128)(2,1)S(1)}, bf16[1,2048,256]{2,1,0:T(8,128)(2,1)}, u32[]{:S(2)}) copy-start(bf16[1,2048,256]{2,1,0:T(8,128)(2,1)} %param.28) | copy-start | bytes 3145732
  9.7 24.6 %copy-start.2 = (bf16[1,256,2048]{2,1,0:T(8,128)(2,1)S(1)}, bf16[1,256,2048]{2,1,0:T(8,128)(2,1)}, u32[]{:S(2)}) copy-start(bf16[1,256,2048]{2,1,0:T(8,128)(2,1)} %param.29) | copy-start | bytes 3145732
  16.4 8.4 %collective-permute-start = (bf16[1,256]{1,0:T(2,128)(2,1)}, bf16[1,256]{1,0:T(2,128)(2,1)S(1)}, u32[]{:S(2)}, u32[]{:S(2)}) collective-permute-start(bf16[1,256]{1,0:T(2,128)(2,1)} %get-tuple-element.34), channel_id=1, source_target_pairs={{0,4},{4,8},{8,12},{12,16},{16,20},{20,24},{24,28},{1,5},{5,9},{9,... | collective-permute-start | bytes 1544 | tf_op jit(solution)/shard_map/ppermute | solution.py:264
  18.9 6.2 %collective-permute-start.1 = (bf16[1,256]{1,0:T(2,128)(2,1)}, bf16[1,256]{1,0:T(2,128)(2,1)S(1)}, u32[]{:S(2)}, u32[]{:S(2)}) collective-permute-start(bf16[1,256]{1,0:T(2,128)(2,1)} %get-tuple-element.35), channel_id=1, source_target_pairs={{4,0},{8,4},{12,8},{16,12},{20,16},{24,20},{28,24},{5,1},{9,5},{13... | collective-permute-start | bytes 1544 | tf_op jit(solution)/shard_map/ppermute | solution.py:265
  20.2 13.4 %collective-permute-start.23 = (bf16[80,2048]{1,0:T(8,128)(2,1)}, bf16[80,2048]{1,0:T(8,128)(2,1)S(1)}, u32[]{:S(2)}, u32[]{:S(2)}) collective-permute-start(bf16[80,2048]{1,0:T(8,128)(2,1)} %get-tuple-element.56), channel_id=1, source_target_pairs={{0,8},{4,12},{8,0},{12,4},{16,24},{20,28},{24,16},{28,20},{1,9},{5... | collective-permute-start | bytes 983048 | tf_op jit(solution)/shard_map/ppermute | solution.py:15
  24.8 17.8 %collective-permute-start.7 = (bf16[2048,256]{1,0:T(8,128)(2,1)S(1)}, bf16[2048,256]{1,0:T(8,128)(2,1)}, u32[]{:S(2)}, u32[]{:S(2)}) collective-permute-start(bf16[2048,256]{1,0:T(8,128)(2,1)S(1)} %bitcast.13), channel_id=1, source_target_pairs={{0,1},{1,0},{2,3},{3,2},{4,5},{5,4},{6,7},{7,6},{8,9},{9,8},{10,11... | collective-permute-start | bytes 3145736 | tf_op jit(solution)/shard_map/ppermute | solution.py:15
  25.0 26.1 %collective-permute-start.8 = (bf16[2048,256]{1,0:T(8,128)(2,1)S(1)}, bf16[2048,256]{1,0:T(8,128)(2,1)}, u32[]{:S(2)}, u32[]{:S(2)}) collective-permute-start(bf16[2048,256]{1,0:T(8,128)(2,1)S(1)} %bitcast.14), channel_id=1, source_target_pairs={{0,2},{1,3},{2,0},{3,1},{4,6},{5,7},{6,4},{7,5},{8,10},{9,11},{10,... | collective-permute-start | bytes 3145736 | tf_op jit(solution)/shard_map/ppermute | solution.py:15
  26.6 71.4 %copy-start.7 = (bf16[80,2048]{1,0:T(8,128)(2,1)}, bf16[80,2048]{1,0:T(8,128)(2,1)S(1)}, u32[]{:S(2)}) copy-start(bf16[80,2048]{1,0:T(8,128)(2,1)S(1)} %collective-permute-done.5.refs_0_) | copy-start | bytes 983044
  26.6 47.1 %collective-permute-start.11 = (bf16[2048,256]{1,0:T(8,128)(2,1)S(1)}, bf16[2048,256]{1,0:T(8,128)(2,1)}, u32[]{:S(2)}, u32[]{:S(2)}) collective-permute-start(bf16[2048,256]{1,0:T(8,128)(2,1)S(1)} %bitcast.18), channel_id=1, source_target_pairs={{0,2},{1,3},{2,0},{3,1},{4,6},{5,7},{6,4},{7,5},{8,10},{9,11},{10,... | collective-permute-start | bytes 3145736 | tf_op jit(solution)/shard_map/ppermute | solution.py:15
  27.1 13.0 %collective-permute-start.24 = (bf16[80,2048]{1,0:T(8,128)(2,1)}, bf16[80,2048]{1,0:T(8,128)(2,1)}, u32[]{:S(2)}, u32[]{:S(2)}) collective-permute-start(bf16[80,2048]{1,0:T(8,128)(2,1)} %get-tuple-element.57), channel_id=1, source_target_pairs={{0,12},{4,8},{8,4},{12,0},{16,28},{20,24},{24,20},{28,16},{1,13},{... | collective-permute-start | bytes 983048 | tf_op jit(solution)/shard_map/ppermute | solution.py:15
  34.3 61.2 %collective-permute-start.14 = (bf16[256,2048]{1,0:T(8,128)(2,1)S(1)}, bf16[256,2048]{1,0:T(8,128)(2,1)}, u32[]{:S(2)}, u32[]{:S(2)}) collective-permute-start(bf16[256,2048]{1,0:T(8,128)(2,1)S(1)} %bitcast.23), channel_id=1, source_target_pairs={{0,2},{1,3},{2,0},{3,1},{4,6},{5,7},{6,4},{7,5},{8,10},{9,11},{10,... | collective-permute-start | bytes 3145736 | tf_op jit(solution)/shard_map/ppermute | solution.py:15
  40.2 2.3 %collective-permute-start.3 = (bf16[160,2048]{1,0:T(8,128)(2,1)}, bf16[160,2048]{1,0:T(8,128)(2,1)S(1)}, u32[]{:S(2)}, u32[]{:S(2)}) collective-permute-start(bf16[160,2048]{1,0:T(8,128)(2,1)} %get-tuple-element.39), channel_id=1, source_target_pairs={{0,1},{1,0},{2,3},{3,2},{4,5},{5,4},{6,7},{7,6},{8,9},{9,8},{10,11... | collective-permute-start | bytes 1966088 | tf_op jit(solution)/shard_map/ppermute | solution.py:15
  42.5 53.0 %copy-start.4 = (bf16[160,2048]{1,0:T(8,128)(2,1)}, bf16[160,2048]{1,0:T(8,128)(2,1)S(1)}, u32[]{:S(2)}) copy-start(bf16[160,2048]{1,0:T(8,128)(2,1)S(1)} %collective-permute-done.3.refs_1_) | copy-start | bytes 1966084
  42.5 55.5 %collective-permute-start.10 = (bf16[2048,256]{1,0:T(8,128)(2,1)S(1)}, bf16[2048,256]{1,0:T(8,128)(2,1)}, u32[]{:S(2)}, u32[]{:S(2)}) collective-permute-start(bf16[2048,256]{1,0:T(8,128)(2,1)S(1)} %bitcast.19), channel_id=1, source_target_pairs={{0,1},{1,0},{2,3},{3,2},{4,5},{5,4},{6,7},{7,6},{8,9},{9,8},{10,11... | collective-permute-start | bytes 3145736 | tf_op jit(solution)/shard_map/ppermute | solution.py:15
  42.6 55.8 %collective-permute-start.13 = (bf16[256,2048]{1,0:T(8,128)(2,1)S(1)}, bf16[256,2048]{1,0:T(8,128)(2,1)}, u32[]{:S(2)}, u32[]{:S(2)}) collective-permute-start(bf16[256,2048]{1,0:T(8,128)(2,1)S(1)} %bitcast.24), channel_id=1, source_target_pairs={{0,1},{1,0},{2,3},{3,2},{4,5},{5,4},{6,7},{7,6},{8,9},{9,8},{10,11... | collective-permute-start | bytes 3145736 | tf_op jit(solution)/shard_map/ppermute | solution.py:15
  51.2 48.8 %collective-permute-start.9 = (bf16[2048,256]{1,0:T(8,128)(2,1)}, bf16[2048,256]{1,0:T(8,128)(2,1)S(1)}, u32[]{:S(2)}, u32[]{:S(2)}) collective-permute-start(bf16[2048,256]{1,0:T(8,128)(2,1)} %collective-permute-done.8.refs_4_.refs_6_), channel_id=1, source_target_pairs={{0,1},{1,0},{2,3},{3,2},{4,5},{5,4},{6,7},{7,6},{8,9},{9,8},{10,11... | collective-permute-start | bytes 3145736 | tf_op jit(solution)/shard_map/ppermute | solution.py:15
  73.7 26.5 %collective-permute-start.12 = (bf16[2048,256]{1,0:T(8,128)(2,1)}, bf16[2048,256]{1,0:T(8,128)(2,1)}, u32[]{:S(2)}, u32[]{:S(2)}) collective-permute-start(bf16[2048,256]{1,0:T(8,128)(2,1)} %collective-permute-done.11.refs_8_.refs_10_), channel_id=1, source_target_pairs={{0,1},{1,0},{2,3},{3,2},{4,5},{5,4},{6,7},{7,6},{8,9},{9,8},{10,11... | collective-permute-start | bytes 3145736 | tf_op jit(solution)/shard_map/ppermute | solution.py:15
  95.5 6.9 %collective-permute-start.15 = (bf16[256,2048]{1,0:T(8,128)(2,1)}, bf16[256,2048]{1,0:T(8,128)(2,1)}, u32[]{:S(2)}, u32[]{:S(2)}) collective-permute-start(bf16[256,2048]{1,0:T(8,128)(2,1)} %collective-permute-done.14.refs_3_), channel_id=1, source_target_pairs={{0,1},{1,0},{2,3},{3,2},{4,5},{5,4},{6,7},{7,6},{8,9},{9,8},{10,11... | collective-permute-start | bytes 3145736 | tf_op jit(solution)/shard_map/ppermute | solution.py:15
  98.0 61.5 %collective-permute-start.2 = (bf16[160,2048]{1,0:T(8,128)(2,1)}, bf16[160,2048]{1,0:T(8,128)(2,1)S(1)}, u32[]{:S(2)}, u32[]{:S(2)}) collective-permute-start(bf16[160,2048]{1,0:T(8,128)(2,1)} %get-tuple-element.37), channel_id=1, source_target_pairs={{0,1},{1,0},{2,3},{3,2},{4,5},{5,4},{6,7},{7,6},{8,9},{9,8},{10,11... | collective-permute-start | bytes 1966088 | tf_op jit(solution)/shard_map/ppermute | solution.py:15
  98.5 62.9 %collective-permute-start.4 = (bf16[160,2048]{1,0:T(8,128)(2,1)}, bf16[160,2048]{1,0:T(8,128)(2,1)S(1)}, u32[]{:S(2)}, u32[]{:S(2)}) collective-permute-start(bf16[160,2048]{1,0:T(8,128)(2,1)} %shard_map.159), channel_id=1, source_target_pairs={{0,2},{1,3},{2,0},{3,1},{4,6},{5,7},{6,4},{7,5},{8,10},{9,11},{10,... | collective-permute-start | bytes 1966088 | tf_op jit(solution)/shard_map/ppermute | solution.py:15
  100.0 32.1 %collective-permute-start.6 = (bf16[80,2048]{1,0:T(8,128)(2,1)}, bf16[80,2048]{1,0:T(8,128)(2,1)S(1)}, u32[]{:S(2)}, u32[]{:S(2)}) collective-permute-start(bf16[80,2048]{1,0:T(8,128)(2,1)} %get-tuple-element.43), channel_id=1, source_target_pairs={{0,20},{4,16},{8,28},{12,24},{16,4},{20,0},{24,12},{28,8},{1,21},{... | collective-permute-start | bytes 983048 | tf_op jit(solution)/shard_map/ppermute | solution.py:15
  100.2 32.5 %collective-permute-start.18 = (bf16[80,2048]{1,0:T(8,128)(2,1)}, bf16[80,2048]{1,0:T(8,128)(2,1)S(1)}, u32[]{:S(2)}, u32[]{:S(2)}) collective-permute-start(bf16[80,2048]{1,0:T(8,128)(2,1)} %get-tuple-element.48), channel_id=1, source_target_pairs={{0,24},{4,28},{8,16},{12,20},{16,8},{20,12},{24,0},{28,4},{1,25},{... | collective-permute-start | bytes 983048 | tf_op jit(solution)/shard_map/ppermute | solution.py:15
  102.4 46.2 %collective-permute-start.19 = (bf16[80,2048]{1,0:T(8,128)(2,1)}, bf16[80,2048]{1,0:T(8,128)(2,1)S(1)}, u32[]{:S(2)}, u32[]{:S(2)}) collective-permute-start(bf16[80,2048]{1,0:T(8,128)(2,1)} %get-tuple-element.49), channel_id=1, source_target_pairs={{0,28},{4,24},{8,20},{12,16},{16,12},{20,8},{24,4},{28,0},{1,29},{... | collective-permute-start | bytes 983048 | tf_op jit(solution)/shard_map/ppermute | solution.py:15
  132.1 31.9 %collective-permute-start.25 = (bf16[80,2048]{1,0:T(8,128)(2,1)}, bf16[80,2048]{1,0:T(8,128)(2,1)S(1)}, u32[]{:S(2)}, u32[]{:S(2)}) collective-permute-start(bf16[80,2048]{1,0:T(8,128)(2,1)} %get-tuple-element.59), channel_id=1, source_target_pairs={{0,4},{4,0},{8,12},{12,8},{16,20},{20,16},{24,28},{28,24},{1,5},{5... | collective-permute-start | bytes 983048 | tf_op jit(solution)/shard_map/ppermute | solution.py:15
  132.6 31.3 %collective-permute-start.26 = (bf16[80,2048]{1,0:T(8,128)(2,1)}, bf16[80,2048]{1,0:T(8,128)(2,1)S(1)}, u32[]{:S(2)}, u32[]{:S(2)}) collective-permute-start(bf16[80,2048]{1,0:T(8,128)(2,1)} %get-tuple-element.60), channel_id=1, source_target_pairs={{0,8},{4,12},{8,0},{12,4},{16,24},{20,28},{24,16},{28,20},{1,9},{5... | collective-permute-start | bytes 983048 | tf_op jit(solution)/shard_map/ppermute | solution.py:15
  148.6 23.2 %collective-permute-start.27 = (bf16[80,2048]{1,0:T(8,128)(2,1)}, bf16[80,2048]{1,0:T(8,128)(2,1)S(1)}, u32[]{:S(2)}, u32[]{:S(2)}) collective-permute-start(bf16[80,2048]{1,0:T(8,128)(2,1)} %get-tuple-element.61), channel_id=1, source_target_pairs={{0,12},{4,8},{8,4},{12,0},{16,28},{20,24},{24,20},{28,16},{1,13},{... | collective-permute-start | bytes 983048 | tf_op jit(solution)/shard_map/ppermute | solution.py:15
  159.5 16.4 %collective-permute-start.20 = (bf16[80,2048]{1,0:T(8,128)(2,1)}, bf16[80,2048]{1,0:T(8,128)(2,1)S(1)}, u32[]{:S(2)}, u32[]{:S(2)}) collective-permute-start(bf16[80,2048]{1,0:T(8,128)(2,1)} %get-tuple-element.50), channel_id=1, source_target_pairs={{0,24},{4,28},{8,16},{12,20},{16,8},{20,12},{24,0},{28,4},{1,25},{... | collective-permute-start | bytes 983048 | tf_op jit(solution)/shard_map/ppermute | solution.py:15
  161.3 18.4 %collective-permute-start.21 = (bf16[80,2048]{1,0:T(8,128)(2,1)}, bf16[80,2048]{1,0:T(8,128)(2,1)S(1)}, u32[]{:S(2)}, u32[]{:S(2)}) collective-permute-start(bf16[80,2048]{1,0:T(8,128)(2,1)} %get-tuple-element.51), channel_id=1, source_target_pairs={{0,28},{4,24},{8,20},{12,16},{16,12},{20,8},{24,4},{28,0},{1,29},{... | collective-permute-start | bytes 983048 | tf_op jit(solution)/shard_map/ppermute | solution.py:15
  163.9 49.1 %collective-permute-start.16 = (bf16[80,2048]{1,0:T(8,128)(2,1)}, bf16[80,2048]{1,0:T(8,128)(2,1)S(1)}, u32[]{:S(2)}, u32[]{:S(2)}) collective-permute-start(bf16[80,2048]{1,0:T(8,128)(2,1)} %get-tuple-element.44), channel_id=1, source_target_pairs={{0,16},{4,20},{8,24},{12,28},{16,0},{20,4},{24,8},{28,12},{1,17},{... | collective-permute-start | bytes 983048 | tf_op jit(solution)/shard_map/ppermute | solution.py:15
  163.9 55.4 %collective-permute-start.17 = (bf16[80,2048]{1,0:T(8,128)(2,1)}, bf16[80,2048]{1,0:T(8,128)(2,1)}, u32[]{:S(2)}, u32[]{:S(2)}) collective-permute-start(bf16[80,2048]{1,0:T(8,128)(2,1)} %get-tuple-element.45), channel_id=1, source_target_pairs={{0,20},{4,16},{8,28},{12,24},{16,4},{20,0},{24,12},{28,8},{1,21},{... | collective-permute-start | bytes 983048 | tf_op jit(solution)/shard_map/ppermute | solution.py:15
  (16 other events, 108.8 us)
where the time goes:
time: 223 us; the launch traced here: 222 us
  waiting for transfers between devices  112 us (50%)
  Pallas kernels  63.2 us (28%)
  starting transfers between devices  43.8 us (20%)
  local copies, waits for them, and re-layouts  2.23 us (1%)
    ppermute x26, waiting for transfers between devices, swapped(): return lax.ppermute(value, axis, [(i, i ^ bit) for i in range(count)])  112 us
    pallas_call x14, Pallas kernels, call(): pl.pallas_call(body, out_shape=outs if single else list(outs), in_specs=[...  56.4 us
    ppermute x26, starting transfers between devices, swapped(): return lax.ppermute(value, axis, [(i, i ^ bit) for i in range(count)])  40.1 us
    pallas_call x1, Pallas kernels, mixer_a(): pl.pallas_call(mixer_a_kernel, grid=(steps,), out_shape=[jax.ShapeDtypeSt...  6.75 us
  transfers between devices with their start and end apart: 28, of which 10 were waited for; matrix products, arithmetic and copies ran while one was open for 0% of the time, Pallas kernels for 26%

commit v1 on v0

--- a/solution.py
+++ b/solution.py
@@ -8,6 +8,7 @@
 
 EPG = 8
 EPSILON = 1e-06
+CHUNKS = 2
 
 
 def swapped(value, axis, bit):
@@ -15,18 +16,20 @@
     return lax.ppermute(value, axis, [(i, i ^ bit) for i in range(count)])
 
 
-def call(body, outs, *operands, scratch=(), smem=0, aliases=None):
+def call(body, outs, *operands, scratch=(), smem=0, limit=16, placed=True):
     vmem = pl.BlockSpec(memory_space=pltpu.VMEM)
     scalar = pl.BlockSpec(memory_space=pltpu.SMEM)
-    single = not isinstance(outs, (list, tuple))
+    near = operands[smem:]
+    if placed:
+        near = [pltpu.with_memory_space_constraint(x, pltpu.VMEM) for x in near]
     return pl.pallas_call(
         body,
-        out_shape=outs if single else list(outs),
-        in_specs=[scalar] * smem + [vmem] * (len(operands) - smem),
-        out_specs=vmem if single else [vmem] * len(outs),
+        out_shape=[pltpu.VMEM(o.shape, o.dtype) for o in outs],
+        in_specs=[scalar] * smem + [vmem] * len(near),
+        out_specs=[vmem] * len(outs),
         scratch_shapes=list(scratch),
-        input_output_aliases=aliases or {},
-    )(*operands)
+        compiler_params=pltpu.CompilerParams(vmem_limit_bytes=limit << 20),
+    )(*operands[:smem], *near)
 
 
 def slots_of(experts, capacity, me, routes_ref):
@@ -112,14 +115,21 @@
         out[...] = answer[i * height : (i + 1) * height]
 
 
-def combine_kernel(blocks, high_ref, low_ref, *refs):
+def combine_kernel(blocks, total, *refs):
     out_ref = refs[-1]
-    rows = jnp.concatenate([r[...] for r in refs[:blocks]], axis=0)
-    total = jnp.dot(high_ref[...], rows, preferred_element_type=jnp.float32)
-    total = total + jnp.dot(low_ref[...], rows, preferred_element_type=jnp.float32)
-    if len(refs) > blocks + 1:
-        total = total + refs[blocks][...]
-    out_ref[...] = total.astype(out_ref.dtype)
+    high_ref, low_ref = refs[:2]
+    rows = jnp.concatenate([r[...] for r in refs[2 : 2 + blocks]], axis=0)
+    value = jnp.dot(high_ref[...], rows, preferred_element_type=jnp.float32)
+    value = value + jnp.dot(low_ref[...], rows, preferred_element_type=jnp.float32)
+    others = refs[2 + blocks : -1]
+    if total:
+        value = value + others[0][...]
+        others = others[1:]
+    start = 0
+    for done in others:
+        out_ref[:, start : start + done.shape[1]] = done[...]
+        start += done.shape[1]
+    out_ref[:, start:] = value.astype(out_ref.dtype)
 
 
 def mixer_a_kernel(rows_ref, gain_ref, value_ref, inner_ref, outer_ref, mixed_ref, gate_ref, top_ref, bottom_ref):
@@ -166,7 +176,7 @@
             whole,
         ],
         out_specs=[piece, piece, edge, edge],
-        name="mixer_a",
+        name="MA",
     )(rows, gain.reshape(1, width), value_weight, inner_gate, outer_gate)
 
 
@@ -236,7 +246,9 @@
 
     gates = gathered_blocks(gate_weight[0], "tp")
     uppers = gathered_blocks(up_weight[0], "tp")
-    downs = gathered_blocks(down_weight[0], "tp")
+    column = width // CHUNKS
+    cut = [down_weight[0][:, c * column : (c + 1) * column] for c in range(CHUNKS)]
+    downs = [gathered_blocks(cut[c], "tp") for c in range(CHUNKS)]
 
     outgoing = call(
         lambda *refs: dispatch_kernel(experts, capacity, *refs),
@@ -246,18 +258,20 @@
         expert_gain.reshape(1, width),
         routes.T,
         smem=1,
+        placed=False,
     )
 
     def exchanged(value):
-        rows = value.reshape(experts, capacity, width)
-        return lax.all_to_all(rows, "ep", split_axis=0, concat_axis=0, tiled=True).reshape(slots, width)
+        rows = value.reshape(experts, capacity, value.shape[1])
+        rows = lax.all_to_all(rows, "ep", split_axis=0, concat_axis=0, tiled=True)
+        return rows.reshape(slots, value.shape[1])
 
     if direct:
         arrived = [outgoing[0]] + [swapped(outgoing[d], "ep", d) for d in range(1, count)]
-        groups = (("near", range(0, 4)), ("far_b", range(6, 8)), ("far_a", range(4, 6)))
+        groups = (("N", range(0, 4)), ("B", range(6, 8)), ("A", range(4, 6)))
     else:
         arrived = [exchanged(outgoing[0])]
-        groups = (("near", range(1)),)
+        groups = (("N", range(1)),)
 
     mixed, gate, top, bottom = mixer_a(mixer_input, mixer_gain, value_weight, inner_gate, outer_gate, split)
     last = experts - 1
@@ -277,23 +291,31 @@
     )
     shares = {name: shares[2 * i : 2 * i + 2] for i, (name, _) in enumerate(ordered)}
 
-    back = {}
+    back = [{} for _ in range(CHUNKS)]
     units = split * gate_weight.shape[2]
+    hiddens = {}
     for name, members in groups:
         n = len(members)
-        hidden = call(
+        (hiddens[name],) = call(
             lambda *refs, n=n: hidden_kernel(n, split, *refs),
-            shaped((n * height, units), bf16),
+            [shaped((n * height, units), bf16)],
             *[arrived[d] for d in members],
             *gates,
             *uppers,
         )
-        answers = call(lambda *refs: down_kernel(split, *refs), [shaped((height, width), bf16)] * n, hidden, *downs)
-        for d, answer in zip(members, answers):
-            if not direct:
-                back[d] = exchanged(answer)
-            else:
-                back[d] = swapped(answer, "ep", d) if d else answer
+    for c in range(CHUNKS):
+        for name, members in groups:
+            answers = call(
+                lambda *refs: down_kernel(split, *refs),
+                [shaped((height, column), bf16)] * len(members),
+                hiddens[name],
+                *downs[c],
+            )
+            for d, answer in zip(members, answers):
+                if not direct:
+                    back[c][d] = exchanged(answer)
+                else:
+                    back[c][d] = swapped(answer, "ep", d) if d else answer
 
     owned = mixed.shape[0] // split
     parts = call(
@@ -315,25 +337,28 @@
         for k in reversed(range(bit, split, 2 * bit)):
             value = addends[k][0]
             if bit > 1:
-                value = call(add_kernel, shaped((owned, width), bf16), *addends[k])
+                (value,) = call(add_kernel, [shaped((owned, width), bf16)], *addends[k])
             addends[k - bit].append(swapped(value, "tp", bit))
         bit *= 2
-    mixer_output = call(add_kernel, shaped((owned, width), bf16), *addends[0])
-
-    total = []
-    for i, (name, members) in enumerate(groups):
-        kind = bf16 if i == len(groups) - 1 else f32
-        blocks = [back[d] for d in members]
-        total = [
-            call(
-                lambda *refs, n=len(blocks): combine_kernel(n, *refs),
-                shaped((local, width), kind),
+    (mixer_output,) = call(add_kernel, [shaped((owned, width), bf16)], *addends[0])
+
+    finished = []
+    for c in range(CHUNKS):
+        total = []
+        for i, (name, members) in enumerate(groups):
+            last = i == len(groups) - 1
+            before = finished if last and c == CHUNKS - 1 else []
+            blocks = [back[c][d] for d in members]
+            total = call(
+                lambda *refs, n=len(blocks), t=len(total): combine_kernel(n, t, *refs),
+                [shaped((local, column * (1 + len(before))), bf16 if last else f32)],
                 *shares[name],
                 *blocks,
                 *total,
+                *before,
             )
-        ]
-    return (mixer_output, total[0])
+        finished = finished + list(total)
+    return (mixer_output, finished[-1])
 
 
 def solution(mesh):

time: 223 us -> 182 us (0.82)
  waiting for transfers between devices: 112 us -> 75.2 us
  Pallas kernels: 63.2 us -> 34.3 us
  local copies, waits for them, and re-layouts: 2.23 us -> 14.8 us
  starting transfers between devices: 43.8 us -> 55.7 us
    ppermute x26 -> x36, waiting for transfers between devices: 112 us -> 69 us  [swapped(): return lax.ppermute(value, axis, [(i, i ^ bit) for i in range(count)])]
    pallas_call x14 -> x20, Pallas kernels: 56.4 us -> 27.6 us  [call(): pl.pallas_call(body, out_shape=[pltpu.VMEM(o.shape, o.dtype) for o in out...]
    ppermute x26 -> x36, starting transfers between devices: 40.1 us -> 51 us  [swapped(): return lax.ppermute(value, axis, [(i, i ^ bit) for i in range(count)])]
    unnamed x40 -> x54, local copies, waits for them, and re-layouts: 2.23 us -> 12.6 us
    ppermute x1, waiting for transfers between devices: 0.14 us -> 4.68 us  [on_device(): below = lax.ppermute(top, 'ep', [(i + 1, i) for i in range(last)])]
    slice x0 -> x1, local copies, waits for them, and re-layouts: none -> 2.25 us  [on_device(): down_weight[0][:, c * column:(c + 1) * column]]
  transfers between devices with their start and end apart: 28 -> 38, of which waited for: 10 -> 13; matrix products, arithmetic and copies ran while one was open for 0% -> 2% of each run, Pallas kernels for 26% -> 18%
where the time goes in v1:
time: 182 us; the launch traced here: 181 us
  waiting for transfers between devices  75.2 us (41%)
  starting transfers between devices  55.7 us (31%)
  Pallas kernels  34.3 us (19%)
  local copies, waits for them, and re-layouts  14.8 us (8%)
    ppermute x36, waiting for transfers between devices, swapped(): return lax.ppermute(value, axis, [(i, i ^ bit) for i in range(count)])  69 us
    ppermute x36, starting transfers between devices, swapped(): return lax.ppermute(value, axis, [(i, i ^ bit) for i in range(count)])  51 us
    pallas_call x20, Pallas kernels, call(): pl.pallas_call(body, out_shape=[pltpu.VMEM(o.shape, o.dtype) for o in out...  27.6 us
    unnamed x54, local copies, waits for them, and re-layouts  12.6 us
    pallas_call x1, Pallas kernels, mixer_a(): pl.pallas_call(mixer_a_kernel, grid=(steps,), out_shape=[jax.ShapeDtypeSt...  6.68 us
    ppermute x1, waiting for transfers between devices, on_device(): below = lax.ppermute(top, 'ep', [(i + 1, i) for i in range(last)])  4.68 us
  transfers between devices with their start and end apart: 38, of which 13 were waited for; matrix products, arithmetic and copies ran while one was open for 2% of the time, Pallas kernels for 18%

profile of v1, /device:TPU:0, one launch (start us, length us, event | category | flops | bytes accessed | tf_op | source)
XLA Modules:
  0.0 181.0 jit_solution(1927104518278302569)
XLA Ops:
  3.1 2.1 %shard_map.162 = (bf16[80,2048]{1,0:T(8,128)(2,1)S(1)}, bf16[80,2048]{1,0:T(8,128)(2,1)}, bf16[80,2048]{1,0:T(8,128)(2,1)}, bf16[80,2048]{1,0:T(8,128)(2,1)S(1)}...) custom-call(s32[1]{0:T(128)} %bitcast.2.refs_0_, ...), custom_call_target="tpu_custom_call" | custom-call | tf_op jit(solution)/shard_map/pallas_call | solution.py:25
  6.7 3.0 %collective-permute-start.22 = (bf16[80,2048]{1,0:T(8,128)(2,1)}, bf16[80,2048]{1,0:T(8,128)(2,1)S(1)}, u32[]{:S(2)}, u32[]{:S(2)}) collective-permute-start(bf16[80,2048]{1,0:T(8,128)(2,1)} %get-tuple-element.63), channel_id=1, source_target_pairs={{0,4},{4,0},{8,12},{12,8},{16,20},{20,16},{24,28},{28,24},{1,5},{5... | collective-permute-start | bytes 983048 | tf_op jit(solution)/shard_map/ppermute | solution.py:16
  9.6 1.6 collective-permute-start.23
  11.2 1.9 %collective-permute-start.11 = (bf16[2048,256]{1,0:T(8,128)(2,1)}, bf16[2048,256]{1,0:T(8,128)(2,1)S(1)}, u32[]{:S(2)}, u32[]{:S(2)}) collective-permute-start(bf16[2048,256]{1,0:T(8,128)(2,1)} %bitcast.15), channel_id=1, source_target_pairs={{0,2},{1,3},{2,0},{3,1},{4,6},{5,7},{6,4},{7,5},{8,10},{9,11},{10,... | collective-permute-start | bytes 3145736 | tf_op jit(solution)/shard_map/ppermute | solution.py:16
  13.2 6.7 %MA.1 = (bf16[640,256]{1,0:T(8,128)(2,1)}, f32[640,256]{1,0:T(8,128)}, bf16[1,256]{1,0:T(2,128)(2,1)}, bf16[1,256]{1,0:T(2,128)(2,1)}) custom-call(bf16[640,2048]{1,0:T(8,128)(2,1)} %rows_ref.1, f32[1,2048]{1,0:T(1,128)} %bitcast.26, bf16[2048,256]{1,0:T(8,128)(2,1)} %value_ref.1, bf16[2048,256]{1,0:T(8,128)(2,1)} %inner_ref.1, bf16[2048,256]{1,0:T(8,128)(2,1)} %outer_ref.1), custom_call_target="tpu_custom_call" | custom-call | tf_op jit(solution)/shard_map/MA/pallas_call | solution.py:162
  19.8 3.4 %collective-permute-start = (bf16[1,256]{1,0:T(2,128)(2,1)}, bf16[1,256]{1,0:T(2,128)(2,1)S(1)}, u32[]{:S(2)}, u32[]{:S(2)}) collective-permute-start(bf16[1,256]{1,0:T(2,128)(2,1)} %get-tuple-element.42), channel_id=1, source_target_pairs={{0,4},{4,8},{8,12},{12,16},{16,20},{20,24},{24,28},{1,5},{5,9},{9,... | collective-permute-start | bytes 1544 | tf_op jit(solution)/shard_map/ppermute | solution.py:278
  26.0 4.7 %collective-permute-done.1.refs_4_ = bf16[1,256]{1,0:T(2,128)(2,1)S(1)} collective-permute-done((bf16[1,256]{1,0:T(2,128)(2,1)}, bf16[1,256]{1,0:T(2,128)(2,1)S(1)}, u32[]{:S(2)}, u32[]{:S(2)}) %collective-permute-start.1) | collective-permute-done | bytes 544 | tf_op jit(solution)/shard_map/ppermute | solution.py:279
  30.7 5.0 %collective-permute-start.18 = (bf16[80,2048]{1,0:T(8,128)(2,1)}, bf16[80,2048]{1,0:T(8,128)(2,1)S(1)}, u32[]{:S(2)}, u32[]{:S(2)}) collective-permute-start(bf16[80,2048]{1,0:T(8,128)(2,1)} %get-tuple-element.56), channel_id=1, source_target_pairs={{0,24},{4,28},{8,16},{12,20},{16,8},{20,12},{24,0},{28,4},{1,25},{... | collective-permute-start | bytes 983048 | tf_op jit(solution)/shard_map/ppermute | solution.py:16
  40.5 2.2 %fusion = (bf16[256,1024]{1,0:T(8,128)(2,1)}, bf16[256,1024]{1,0:T(8,128)(2,1)}) fusion(bf16[256,2048]{1,0:T(8,128)(2,1)} %bitcast.25), kind=kLoop, calls=%fused_computation | loop fusion | bytes 2097152 | tf_op jit(solution)/shard_map/slice | solution.py:250
  42.8 1.7 collective-permute-done.18.refs_0_
  46.4 5.8 %collective-permute-done.19.refs_1_ = bf16[80,2048]{1,0:T(8,128)(2,1)S(1)} collective-permute-done((bf16[80,2048]{1,0:T(8,128)(2,1)}, bf16[80,2048]{1,0:T(8,128)(2,1)S(1)}, u32[]{:S(2)}, u32[]{:S(2)}) %collective-permute-start.19) | collective-permute-done | bytes 327712 | tf_op jit(solution)/shard_map/ppermute | solution.py:16
  52.9 22.6 %collective-permute-done.5.refs_0_ = bf16[80,2048]{1,0:T(8,128)(2,1)S(1)} collective-permute-done((bf16[80,2048]{1,0:T(8,128)(2,1)}, bf16[80,2048]{1,0:T(8,128)(2,1)S(1)}, u32[]{:S(2)}, u32[]{:S(2)}) %collective-permute-start.5) | collective-permute-done | bytes 327712 | tf_op jit(solution)/shard_map/ppermute | solution.py:16
  82.2 6.6 %collective-permute-done.14.refs_3_ = bf16[256,1024]{1,0:T(8,128)(2,1)} collective-permute-done((bf16[256,1024]{1,0:T(8,128)(2,1)}, bf16[256,1024]{1,0:T(8,128)(2,1)}, u32[]{:S(2)}, u32[]{:S(2)}) %collective-permute-start.14) | collective-permute-done | bytes 524320 | tf_op jit(solution)/shard_map/ppermute | solution.py:16
  91.6 3.6 %collective-permute-done.30.refs_4_ = bf16[256,1024]{1,0:T(8,128)(2,1)S(1)} collective-permute-done((bf16[256,1024]{1,0:T(8,128)(2,1)}, bf16[256,1024]{1,0:T(8,128)(2,1)S(1)}, u32[]{:S(2)}, u32[]{:S(2)}) %collective-permute-start.30) | collective-permute-done | bytes 524320 | tf_op jit(solution)/shard_map/ppermute | solution.py:16
  97.3 2.9 %shard_map.165.refs_0_ = bf16[160,1024]{1,0:T(8,128)(2,1)S(1)} custom-call(bf16[80,2048]{1,0:T(8,128)(2,1)S(1)} %copy-done.14, bf16[80,2048]{1,0:T(8,128)(2,1)S(1)} %copy-done.16, bf16[2048,256]{1,0:T(8,128)(2,1)S(1)} %bitcast.12, bf16[2048,256]{1,0:T(8,128)(2,1)S(1)} %collective-permute-done.7.refs_3_.refs_5_, ...), custom_call_target="tpu_custom_call" | custom-call | tf_op jit(solution)/shard_map/pallas_call | solution.py:25
  100.2 4.1 %shard_map.167.refs_0_ = bf16[320,1024]{1,0:T(8,128)(2,1)S(1)} custom-call(bf16[80,2048]{1,0:T(8,128)(2,1)S(1)} %copy-done.6, bf16[80,2048]{1,0:T(8,128)(2,1)S(1)} %copy-done.8, bf16[80,2048]{1,0:T(8,128)(2,1)S(1)} %copy-done.10, bf16[80,2048]{1,0:T(8,128)(2,1)S(1)} %copy-done.12, bf16[2048,256]{1,0:T(8,128)(2,1)S(1)} %bitcast.13, ...), custom_call_target="tpu_custom_call" | custom-call | tf_op jit(solution)/shard_map/pallas_call | solution.py:25
  104.3 2.2 %shard_map.173 = (bf16[80,1024]{1,0:T(8,128)(2,1)S(1)}, bf16[80,1024]{1,0:T(8,128)(2,1)S(1)}, bf16[80,1024]{1,0:T(8,128)(2,1)S(1)}, bf16[80,1024]{1,0:T(8,128)(2,1)S(1)}) custom-call(bf16[320,1024]{1,0:T(8,128)(2,1)S(1)} %shard_map.167.refs_0_, bf16[256,1024]{1,0:T(8,128)(2,1)} %get-tuple-element.78.refs_1_, ...), custom_call_target="tpu_custom_call" | custom-call | tf_op jit(solution)/shard_map/pallas_call | solution.py:25
  106.5 1.9 %shard_map.172 = (bf16[80,1024]{1,0:T(8,128)(2,1)S(1)}, bf16[80,1024]{1,0:T(8,128)(2,1)S(1)}) custom-call(bf16[160,1024]{1,0:T(8,128)(2,1)S(1)} %shard_map.165.refs_0_, bf16[256,1024]{1,0:T(8,128)(2,1)} %get-tuple-element.78.refs_1_, bf16[256,1024]{1,0:T(8,128)(2,1)} %collective-permute-done.28.refs_2_, bf16[256,1024]{1,0:T(8,128)(2,1)} %collective-permute-done.29.refs_3_, ...), custom_call_target="tpu_custom_call" | custom-call | tf_op jit(solution)/shard_map/pallas_call | solution.py:25
  108.4 6.8 %collective-permute-done.6.refs_1_ = bf16[80,2048]{1,0:T(8,128)(2,1)S(1)} collective-permute-done((bf16[80,2048]{1,0:T(8,128)(2,1)S(1)}, bf16[80,2048]{1,0:T(8,128)(2,1)S(1)}, u32[]{:S(2)}, u32[]{:S(2)}) %collective-permute-start.6) | collective-permute-done | bytes 327712 | tf_op jit(solution)/shard_map/ppermute | solution.py:16
  116.1 2.7 %collective-permute-start.37 = (bf16[80,1024]{1,0:T(8,128)(2,1)S(1)}, bf16[80,1024]{1,0:T(8,128)(2,1)S(1)}, u32[]{:S(2)}, u32[]{:S(2)}) collective-permute-start(bf16[80,1024]{1,0:T(8,128)(2,1)S(1)} %get-tuple-element.77), channel_id=1, source_target_pairs={{0,12},{4,8},{8,4},{12,0},{16,28},{20,24},{24,20},{28,16},{1,13},{... | collective-permute-start | bytes 491528 | tf_op jit(solution)/shard_map/ppermute | solution.py:16
  119.2 2.0 %shard_map.168 = (bf16[80,1024]{1,0:T(8,128)(2,1)S(1)}, bf16[80,1024]{1,0:T(8,128)(2,1)S(1)}, bf16[80,1024]{1,0:T(8,128)(2,1)S(1)}, bf16[80,1024]{1,0:T(8,128)(2,1)S(1)}) custom-call(bf16[320,1024]{1,0:T(8,128)(2,1)S(1)} %shard_map.167.refs_0_, bf16[256,1024]{1,0:T(8,128)(2,1)} %get-tuple-element.79.refs_1_, ...), custom_call_target="tpu_custom_call" | custom-call | tf_op jit(solution)/shard_map/pallas_call | solution.py:25
  121.3 1.7 shard_map.166
  123.0 3.7 %collective-permute-start.34 = (bf16[80,1024]{1,0:T(8,128)(2,1)S(1)}, bf16[80,1024]{1,0:T(8,128)(2,1)S(1)}, u32[]{:S(2)}, u32[]{:S(2)}) collective-permute-start(bf16[80,1024]{1,0:T(8,128)(2,1)S(1)} %get-tuple-element.73), channel_id=1, source_target_pairs={{0,28},{4,24},{8,20},{12,16},{16,12},{20,8},{24,4},{28,0},{1,29},{... | collective-permute-start | bytes 491528 | tf_op jit(solution)/shard_map/ppermute | solution.py:16
  127.9 6.4 %collective-permute-done.37.refs_5_ = bf16[80,1024]{1,0:T(8,128)(2,1)S(1)} collective-permute-done((bf16[80,1024]{1,0:T(8,128)(2,1)S(1)}, bf16[80,1024]{1,0:T(8,128)(2,1)S(1)}, u32[]{:S(2)}, u32[]{:S(2)}) %collective-permute-start.37) | collective-permute-done | bytes 163872 | tf_op jit(solution)/shard_map/ppermute | solution.py:16
  134.3 2.8 %shard_map.163.refs_0_ = bf16[160,1024]{1,0:T(8,128)(2,1)S(1)} custom-call(bf16[80,2048]{1,0:T(8,128)(2,1)S(1)} %collective-permute-done.5.refs_0_, bf16[80,2048]{1,0:T(8,128)(2,1)S(1)} %collective-permute-done.6.refs_1_, bf16[2048,256]{1,0:T(8,128)(2,1)S(1)} %bitcast.14, bf16[2048,256]{1,0:T(8,128)(2,1)S(1)} %collective-permute-done.7.refs_3_.refs_5_, ...), custom_call_target="tpu_custom_call" | custom-call | tf_op jit(solution)/shard_map/pallas_call | solution.py:25
  137.1 1.9 %shard_map.171 = (bf16[80,1024]{1,0:T(8,128)(2,1)S(1)}, bf16[80,1024]{1,0:T(8,128)(2,1)S(1)}) custom-call(bf16[160,1024]{1,0:T(8,128)(2,1)S(1)} %shard_map.163.refs_0_, bf16[256,1024]{1,0:T(8,128)(2,1)} %get-tuple-element.78.refs_1_, bf16[256,1024]{1,0:T(8,128)(2,1)} %collective-permute-done.28.refs_2_, bf16[256,1024]{1,0:T(8,128)(2,1)} %collective-permute-done.29.refs_3_, ...), custom_call_target="tpu_custom_call" | custom-call | tf_op jit(solution)/shard_map/pallas_call | solution.py:25
  139.0 1.7 shard_map.164
  140.8 2.6 %collective-permute-start.31 = (bf16[80,1024]{1,0:T(8,128)(2,1)S(1)}, bf16[80,1024]{1,0:T(8,128)(2,1)S(1)}, u32[]{:S(2)}, u32[]{:S(2)}) collective-permute-start(bf16[80,1024]{1,0:T(8,128)(2,1)S(1)} %get-tuple-element.70), channel_id=1, source_target_pairs={{0,16},{4,20},{8,24},{12,28},{16,0},{20,4},{24,8},{28,12},{1,17},{... | collective-permute-start | bytes 491528 | tf_op jit(solution)/shard_map/ppermute | solution.py:16
  143.3 2.8 %collective-permute-start.21 = (bf16[80,1024]{1,0:T(8,128)(2,1)S(1)}, bf16[80,1024]{1,0:T(8,128)(2,1)S(1)}, u32[]{:S(2)}, u32[]{:S(2)}) collective-permute-start(bf16[80,1024]{1,0:T(8,128)(2,1)S(1)} %get-tuple-element.59), channel_id=1, source_target_pairs={{0,28},{4,24},{8,20},{12,16},{16,12},{20,8},{24,4},{28,0},{1,29},{... | collective-permute-start | bytes 491528 | tf_op jit(solution)/shard_map/ppermute | solution.py:16
  148.6 13.9 %collective-permute-start.17 = (bf16[80,1024]{1,0:T(8,128)(2,1)S(1)}, bf16[80,1024]{1,0:T(8,128)(2,1)S(1)}, u32[]{:S(2)}, u32[]{:S(2)}) collective-permute-start(bf16[80,1024]{1,0:T(8,128)(2,1)S(1)} %get-tuple-element.53), channel_id=1, source_target_pairs={{0,20},{4,16},{8,28},{12,24},{16,4},{20,0},{24,12},{28,8},{1,21},{... | collective-permute-start | bytes 491528 | tf_op jit(solution)/shard_map/ppermute | solution.py:16
  165.6 8.8 %collective-permute-done.32.refs_3_ = bf16[80,1024]{1,0:T(8,128)(2,1)S(1)} collective-permute-done((bf16[80,1024]{1,0:T(8,128)(2,1)S(1)}, bf16[80,1024]{1,0:T(8,128)(2,1)S(1)}, u32[]{:S(2)}, u32[]{:S(2)}) %collective-permute-start.32) | collective-permute-done | bytes 163872 | tf_op jit(solution)/shard_map/ppermute | solution.py:16
  176.2 3.7 %collective-permute-done.17.refs_3_ = bf16[80,1024]{1,0:T(8,128)(2,1)S(1)} collective-permute-done((bf16[80,1024]{1,0:T(8,128)(2,1)S(1)}, bf16[80,1024]{1,0:T(8,128)(2,1)S(1)}, u32[]{:S(2)}, u32[]{:S(2)}) %collective-permute-start.17) | collective-permute-done | bytes 163872 | tf_op jit(solution)/shard_map/ppermute | solution.py:16
  (120 shorter events, 36.7 us)
Async XLA Ops:
  6.7 29.0 %collective-permute-start.22 = (bf16[80,2048]{1,0:T(8,128)(2,1)}, bf16[80,2048]{1,0:T(8,128)(2,1)S(1)}, u32[]{:S(2)}, u32[]{:S(2)}) collective-permute-start(bf16[80,2048]{1,0:T(8,128)(2,1)} %get-tuple-element.63), channel_id=1, source_target_pairs={{0,4},{4,0},{8,12},{12,8},{16,20},{20,16},{24,28},{28,24},{1,5},{5... | collective-permute-start | bytes 983048 | tf_op jit(solution)/shard_map/ppermute | solution.py:16
  9.6 28.0 %collective-permute-start.23 = (bf16[80,2048]{1,0:T(8,128)(2,1)}, bf16[80,2048]{1,0:T(8,128)(2,1)S(1)}, u32[]{:S(2)}, u32[]{:S(2)}) collective-permute-start(bf16[80,2048]{1,0:T(8,128)(2,1)} %get-tuple-element.64), channel_id=1, source_target_pairs={{0,8},{4,12},{8,0},{12,4},{16,24},{20,28},{24,16},{28,20},{1,9},{5... | collective-permute-start | bytes 983048 | tf_op jit(solution)/shard_map/ppermute | solution.py:16
  11.2 27.8 %collective-permute-start.24 = (bf16[80,2048]{1,0:T(8,128)(2,1)S(1)}, bf16[80,2048]{1,0:T(8,128)(2,1)S(1)}, u32[]{:S(2)}, u32[]{:S(2)}) collective-permute-start(bf16[80,2048]{1,0:T(8,128)(2,1)S(1)} %get-tuple-element.65), channel_id=1, source_target_pairs={{0,12},{4,8},{8,4},{12,0},{16,28},{20,24},{24,20},{28,16},{1,13},{... | collective-permute-start | bytes 983048 | tf_op jit(solution)/shard_map/ppermute | solution.py:16
  11.2 77.6 %collective-permute-start.11 = (bf16[2048,256]{1,0:T(8,128)(2,1)}, bf16[2048,256]{1,0:T(8,128)(2,1)S(1)}, u32[]{:S(2)}, u32[]{:S(2)}) collective-permute-start(bf16[2048,256]{1,0:T(8,128)(2,1)} %bitcast.15), channel_id=1, source_target_pairs={{0,2},{1,3},{2,0},{3,1},{4,6},{5,7},{6,4},{7,5},{8,10},{9,11},{10,... | collective-permute-start | bytes 3145736 | tf_op jit(solution)/shard_map/ppermute | solution.py:16
  30.7 13.8 %collective-permute-start.18 = (bf16[80,2048]{1,0:T(8,128)(2,1)}, bf16[80,2048]{1,0:T(8,128)(2,1)S(1)}, u32[]{:S(2)}, u32[]{:S(2)}) collective-permute-start(bf16[80,2048]{1,0:T(8,128)(2,1)} %get-tuple-element.56), channel_id=1, source_target_pairs={{0,24},{4,28},{8,16},{12,20},{16,8},{20,12},{24,0},{28,4},{1,25},{... | collective-permute-start | bytes 983048 | tf_op jit(solution)/shard_map/ppermute | solution.py:16
  36.4 15.8 %collective-permute-start.19 = (bf16[80,2048]{1,0:T(8,128)(2,1)}, bf16[80,2048]{1,0:T(8,128)(2,1)S(1)}, u32[]{:S(2)}, u32[]{:S(2)}) collective-permute-start(bf16[80,2048]{1,0:T(8,128)(2,1)} %get-tuple-element.57), channel_id=1, source_target_pairs={{0,28},{4,24},{8,20},{12,16},{16,12},{20,8},{24,4},{28,0},{1,29},{... | collective-permute-start | bytes 983048 | tf_op jit(solution)/shard_map/ppermute | solution.py:16
  38.4 51.0 %collective-permute-start.8 = (bf16[2048,256]{1,0:T(8,128)(2,1)S(1)}, bf16[2048,256]{1,0:T(8,128)(2,1)}, u32[]{:S(2)}, u32[]{:S(2)}) collective-permute-start(bf16[2048,256]{1,0:T(8,128)(2,1)S(1)} %bitcast.10), channel_id=1, source_target_pairs={{0,2},{1,3},{2,0},{3,1},{4,6},{5,7},{6,4},{7,5},{8,10},{9,11},{10,... | collective-permute-start | bytes 3145736 | tf_op jit(solution)/shard_map/ppermute | solution.py:16
  39.8 35.7 %collective-permute-start.5 = (bf16[80,2048]{1,0:T(8,128)(2,1)}, bf16[80,2048]{1,0:T(8,128)(2,1)S(1)}, u32[]{:S(2)}, u32[]{:S(2)}) collective-permute-start(bf16[80,2048]{1,0:T(8,128)(2,1)} %get-tuple-element.50), channel_id=1, source_target_pairs={{0,16},{4,20},{8,24},{12,28},{16,0},{20,4},{24,8},{28,12},{1,17},{... | collective-permute-start | bytes 983048 | tf_op jit(solution)/shard_map/ppermute | solution.py:16
  45.2 36.4 %collective-permute-start.29 = (bf16[256,1024]{1,0:T(8,128)(2,1)}, bf16[256,1024]{1,0:T(8,128)(2,1)}, u32[]{:S(2)}, u32[]{:S(2)}) collective-permute-start(bf16[256,1024]{1,0:T(8,128)(2,1)} %get-tuple-element.78.refs_1_), channel_id=1, source_target_pairs={{0,2},{1,3},{2,0},{3,1},{4,6},{5,7},{6,4},{7,5},{8,10},{9,11},{10,... | collective-permute-start | bytes 1572872 | tf_op jit(solution)/shard_map/ppermute | solution.py:16
  52.9 28.8 %collective-permute-start.28 = (bf16[256,1024]{1,0:T(8,128)(2,1)}, bf16[256,1024]{1,0:T(8,128)(2,1)}, u32[]{:S(2)}, u32[]{:S(2)}) collective-permute-start(bf16[256,1024]{1,0:T(8,128)(2,1)} %get-tuple-element.78.refs_1_), channel_id=1, source_target_pairs={{0,1},{1,0},{2,3},{3,2},{4,5},{5,4},{6,7},{7,6},{8,9},{9,8},{10,11... | collective-permute-start | bytes 1572872 | tf_op jit(solution)/shard_map/ppermute | solution.py:16
  75.5 13.3 %collective-permute-start.14 = (bf16[256,1024]{1,0:T(8,128)(2,1)}, bf16[256,1024]{1,0:T(8,128)(2,1)}, u32[]{:S(2)}, u32[]{:S(2)}) collective-permute-start(bf16[256,1024]{1,0:T(8,128)(2,1)} %get-tuple-element.79.refs_1_), channel_id=1, source_target_pairs={{0,2},{1,3},{2,0},{3,1},{4,6},{5,7},{6,4},{7,5},{8,10},{9,11},{10,... | collective-permute-start | bytes 1572872 | tf_op jit(solution)/shard_map/ppermute | solution.py:16
  81.7 8.2 %collective-permute-start.10 = (bf16[2048,256]{1,0:T(8,128)(2,1)S(1)}, bf16[2048,256]{1,0:T(8,128)(2,1)S(1)}, u32[]{:S(2)}, u32[]{:S(2)}) collective-permute-start(bf16[2048,256]{1,0:T(8,128)(2,1)S(1)} %bitcast.16), channel_id=1, source_target_pairs={{0,1},{1,0},{2,3},{3,2},{4,5},{5,4},{6,7},{7,6},{8,9},{9,8},{10,11... | collective-permute-start | bytes 3145736 | tf_op jit(solution)/shard_map/ppermute | solution.py:16
  89.3 7.7 %collective-permute-start.9 = (bf16[2048,256]{1,0:T(8,128)(2,1)}, bf16[2048,256]{1,0:T(8,128)(2,1)S(1)}, u32[]{:S(2)}, u32[]{:S(2)}) collective-permute-start(bf16[2048,256]{1,0:T(8,128)(2,1)} %collective-permute-done.8.refs_4_.refs_6_), channel_id=1, source_target_pairs={{0,1},{1,0},{2,3},{3,2},{4,5},{5,4},{6,7},{7,6},{8,9},{9,8},{10,11... | collective-permute-start | bytes 3145736 | tf_op jit(solution)/shard_map/ppermute | solution.py:16
  89.9 26.2 %collective-permute-start.2 = (bf16[160,2048]{1,0:T(8,128)(2,1)S(1)}, bf16[160,2048]{1,0:T(8,128)(2,1)S(1)}, u32[]{:S(2)}, u32[]{:S(2)}) collective-permute-start(bf16[160,2048]{1,0:T(8,128)(2,1)S(1)} %get-tuple-element.45), channel_id=1, source_target_pairs={{0,1},{1,0},{2,3},{3,2},{4,5},{5,4},{6,7},{7,6},{8,9},{9,8},{10,11... | collective-permute-start | bytes 1966088 | tf_op jit(solution)/shard_map/ppermute | solution.py:16
  91.5 24.6 %collective-permute-start.13 = (bf16[256,1024]{1,0:T(8,128)(2,1)}, bf16[256,1024]{1,0:T(8,128)(2,1)S(1)}, u32[]{:S(2)}, u32[]{:S(2)}) collective-permute-start(bf16[256,1024]{1,0:T(8,128)(2,1)} %get-tuple-element.79.refs_1_), channel_id=1, source_target_pairs={{0,1},{1,0},{2,3},{3,2},{4,5},{5,4},{6,7},{7,6},{8,9},{9,8},{10,11... | collective-permute-start | bytes 1572872 | tf_op jit(solution)/shard_map/ppermute | solution.py:16
  95.2 23.5 %collective-permute-start.15 = (bf16[256,1024]{1,0:T(8,128)(2,1)}, bf16[256,1024]{1,0:T(8,128)(2,1)S(1)}, u32[]{:S(2)}, u32[]{:S(2)}) collective-permute-start(bf16[256,1024]{1,0:T(8,128)(2,1)} %collective-permute-done.14.refs_3_), channel_id=1, source_target_pairs={{0,1},{1,0},{2,3},{3,2},{4,5},{5,4},{6,7},{7,6},{8,9},{9,8},{10,11... | collective-permute-start | bytes 1572872 | tf_op jit(solution)/shard_map/ppermute | solution.py:16
  95.5 27.5 %collective-permute-start.4 = (bf16[160,2048]{1,0:T(8,128)(2,1)S(1)}, bf16[160,2048]{1,0:T(8,128)(2,1)S(1)}, u32[]{:S(2)}, u32[]{:S(2)}) collective-permute-start(bf16[160,2048]{1,0:T(8,128)(2,1)S(1)} %shard_map.159), channel_id=1, source_target_pairs={{0,2},{1,3},{2,0},{3,1},{4,6},{5,7},{6,4},{7,5},{8,10},{9,11},{10,... | collective-permute-start | bytes 1966088 | tf_op jit(solution)/shard_map/ppermute | solution.py:16
  97.1 18.1 %collective-permute-start.6 = (bf16[80,2048]{1,0:T(8,128)(2,1)S(1)}, bf16[80,2048]{1,0:T(8,128)(2,1)S(1)}, u32[]{:S(2)}, u32[]{:S(2)}) collective-permute-start(bf16[80,2048]{1,0:T(8,128)(2,1)S(1)} %copy-done.25), channel_id=1, source_target_pairs={{0,20},{4,16},{8,28},{12,24},{16,4},{20,0},{24,12},{28,8},{1,21},{... | collective-permute-start | bytes 983048 | tf_op jit(solution)/shard_map/ppermute | solution.py:16
  115.2 11.4 %collective-permute-start.35 = (bf16[80,1024]{1,0:T(8,128)(2,1)S(1)}, bf16[80,1024]{1,0:T(8,128)(2,1)S(1)}, u32[]{:S(2)}, u32[]{:S(2)}) collective-permute-start(bf16[80,1024]{1,0:T(8,128)(2,1)S(1)} %get-tuple-element.75), channel_id=1, source_target_pairs={{0,4},{4,0},{8,12},{12,8},{16,20},{20,16},{24,28},{28,24},{1,5},{5... | collective-permute-start | bytes 491528 | tf_op jit(solution)/shard_map/ppermute | solution.py:16
  116.1 11.8 %collective-permute-start.36 = (bf16[80,1024]{1,0:T(8,128)(2,1)S(1)}, bf16[80,1024]{1,0:T(8,128)(2,1)S(1)}, u32[]{:S(2)}, u32[]{:S(2)}) collective-permute-start(bf16[80,1024]{1,0:T(8,128)(2,1)S(1)} %get-tuple-element.76), channel_id=1, source_target_pairs={{0,8},{4,12},{8,0},{12,4},{16,24},{20,28},{24,16},{28,20},{1,9},{5... | collective-permute-start | bytes 491528 | tf_op jit(solution)/shard_map/ppermute | solution.py:16
  116.1 18.2 %collective-permute-start.37 = (bf16[80,1024]{1,0:T(8,128)(2,1)S(1)}, bf16[80,1024]{1,0:T(8,128)(2,1)S(1)}, u32[]{:S(2)}, u32[]{:S(2)}) collective-permute-start(bf16[80,1024]{1,0:T(8,128)(2,1)S(1)} %get-tuple-element.77), channel_id=1, source_target_pairs={{0,12},{4,8},{8,4},{12,0},{16,28},{20,24},{24,20},{28,16},{1,13},{... | collective-permute-start | bytes 491528 | tf_op jit(solution)/shard_map/ppermute | solution.py:16
  118.7 15.6 %collective-permute-start.33 = (bf16[80,1024]{1,0:T(8,128)(2,1)S(1)}, bf16[80,1024]{1,0:T(8,128)(2,1)S(1)}, u32[]{:S(2)}, u32[]{:S(2)}) collective-permute-start(bf16[80,1024]{1,0:T(8,128)(2,1)S(1)} %get-tuple-element.72), channel_id=1, source_target_pairs={{0,24},{4,28},{8,16},{12,20},{16,8},{20,12},{24,0},{28,4},{1,25},{... | collective-permute-start | bytes 491528 | tf_op jit(solution)/shard_map/ppermute | solution.py:16
  123.0 17.8 %collective-permute-start.34 = (bf16[80,1024]{1,0:T(8,128)(2,1)S(1)}, bf16[80,1024]{1,0:T(8,128)(2,1)S(1)}, u32[]{:S(2)}, u32[]{:S(2)}) collective-permute-start(bf16[80,1024]{1,0:T(8,128)(2,1)S(1)} %get-tuple-element.73), channel_id=1, source_target_pairs={{0,28},{4,24},{8,20},{12,16},{16,12},{20,8},{24,4},{28,0},{1,29},{... | collective-permute-start | bytes 491528 | tf_op jit(solution)/shard_map/ppermute | solution.py:16
  126.7 16.7 %collective-permute-start.25 = (bf16[80,1024]{1,0:T(8,128)(2,1)S(1)}, bf16[80,1024]{1,0:T(8,128)(2,1)S(1)}, u32[]{:S(2)}, u32[]{:S(2)}) collective-permute-start(bf16[80,1024]{1,0:T(8,128)(2,1)S(1)} %get-tuple-element.67), channel_id=1, source_target_pairs={{0,4},{4,0},{8,12},{12,8},{16,20},{20,16},{24,28},{28,24},{1,5},{5... | collective-permute-start | bytes 491528 | tf_op jit(solution)/shard_map/ppermute | solution.py:16
  127.9 18.2 %collective-permute-start.26 = (bf16[80,1024]{1,0:T(8,128)(2,1)S(1)}, bf16[80,1024]{1,0:T(8,128)(2,1)S(1)}, u32[]{:S(2)}, u32[]{:S(2)}) collective-permute-start(bf16[80,1024]{1,0:T(8,128)(2,1)S(1)} %get-tuple-element.68), channel_id=1, source_target_pairs={{0,8},{4,12},{8,0},{12,4},{16,24},{20,28},{24,16},{28,20},{1,9},{5... | collective-permute-start | bytes 491528 | tf_op jit(solution)/shard_map/ppermute | solution.py:16
  134.3 13.3 %collective-permute-start.27 = (bf16[80,1024]{1,0:T(8,128)(2,1)S(1)}, bf16[80,1024]{1,0:T(8,128)(2,1)S(1)}, u32[]{:S(2)}, u32[]{:S(2)}) collective-permute-start(bf16[80,1024]{1,0:T(8,128)(2,1)S(1)} %get-tuple-element.69), channel_id=1, source_target_pairs={{0,12},{4,8},{8,4},{12,0},{16,28},{20,24},{24,20},{28,16},{1,13},{... | collective-permute-start | bytes 491528 | tf_op jit(solution)/shard_map/ppermute | solution.py:16
  134.3 14.2 %collective-permute-start.20 = (bf16[80,1024]{1,0:T(8,128)(2,1)S(1)}, bf16[80,1024]{1,0:T(8,128)(2,1)S(1)}, u32[]{:S(2)}, u32[]{:S(2)}) collective-permute-start(bf16[80,1024]{1,0:T(8,128)(2,1)S(1)} %get-tuple-element.58), channel_id=1, source_target_pairs={{0,24},{4,28},{8,16},{12,20},{16,8},{20,12},{24,0},{28,4},{1,25},{... | collective-permute-start | bytes 491528 | tf_op jit(solution)/shard_map/ppermute | solution.py:16
  140.8 24.9 %collective-permute-start.31 = (bf16[80,1024]{1,0:T(8,128)(2,1)S(1)}, bf16[80,1024]{1,0:T(8,128)(2,1)S(1)}, u32[]{:S(2)}, u32[]{:S(2)}) collective-permute-start(bf16[80,1024]{1,0:T(8,128)(2,1)S(1)} %get-tuple-element.70), channel_id=1, source_target_pairs={{0,16},{4,20},{8,24},{12,28},{16,0},{20,4},{24,8},{28,12},{1,17},{... | collective-permute-start | bytes 491528 | tf_op jit(solution)/shard_map/ppermute | solution.py:16
  143.3 22.0 %collective-permute-start.21 = (bf16[80,1024]{1,0:T(8,128)(2,1)S(1)}, bf16[80,1024]{1,0:T(8,128)(2,1)S(1)}, u32[]{:S(2)}, u32[]{:S(2)}) collective-permute-start(bf16[80,1024]{1,0:T(8,128)(2,1)S(1)} %get-tuple-element.59), channel_id=1, source_target_pairs={{0,28},{4,24},{8,20},{12,16},{16,12},{20,8},{24,4},{28,0},{1,29},{... | collective-permute-start | bytes 491528 | tf_op jit(solution)/shard_map/ppermute | solution.py:16
  146.1 28.3 %collective-permute-start.32 = (bf16[80,1024]{1,0:T(8,128)(2,1)S(1)}, bf16[80,1024]{1,0:T(8,128)(2,1)S(1)}, u32[]{:S(2)}, u32[]{:S(2)}) collective-permute-start(bf16[80,1024]{1,0:T(8,128)(2,1)S(1)} %get-tuple-element.71), channel_id=1, source_target_pairs={{0,20},{4,16},{8,28},{12,24},{16,4},{20,0},{24,12},{28,8},{1,21},{... | collective-permute-start | bytes 491528 | tf_op jit(solution)/shard_map/ppermute | solution.py:16
  147.6 28.6 %collective-permute-start.16 = (bf16[80,1024]{1,0:T(8,128)(2,1)S(1)}, bf16[80,1024]{1,0:T(8,128)(2,1)S(1)}, u32[]{:S(2)}, u32[]{:S(2)}) collective-permute-start(bf16[80,1024]{1,0:T(8,128)(2,1)S(1)} %get-tuple-element.52), channel_id=1, source_target_pairs={{0,16},{4,20},{8,24},{12,28},{16,0},{20,4},{24,8},{28,12},{1,17},{... | collective-permute-start | bytes 491528 | tf_op jit(solution)/shard_map/ppermute | solution.py:16
  148.6 31.3 %collective-permute-start.17 = (bf16[80,1024]{1,0:T(8,128)(2,1)S(1)}, bf16[80,1024]{1,0:T(8,128)(2,1)S(1)}, u32[]{:S(2)}, u32[]{:S(2)}) collective-permute-start(bf16[80,1024]{1,0:T(8,128)(2,1)S(1)} %get-tuple-element.53), channel_id=1, source_target_pairs={{0,20},{4,16},{8,28},{12,24},{16,4},{20,0},{24,12},{28,8},{1,21},{... | collective-permute-start | bytes 491528 | tf_op jit(solution)/shard_map/ppermute | solution.py:16
  (32 other events, 254.1 us)
